TPU v7x, 32 devices: a whole 2x2x4 slice. The times are simulated.
32 devices in a mesh: kv: 8 (over z, y), tp: 4 (over x, core).
Axes of the slice: x: 2, y: 2, z: 4, core: 2. Of those that a mesh axis runs over, the one named last changes fastest.
Arguments:
- tokens: bfloat16 [6144, 2048], P('kv'), may hold values from -6 to 6
- w_query: bfloat16 [2048, 4096], P(None, 'tp'), may hold values from -3.1819805 to 3.1819805
- w_latent: bfloat16 [2048, 256], replicated, may hold values from -0.13258252 to 0.13258252
- latent_gain: float32 [256], replicated, may hold values from 0.1 to 1.9
- w_output: bfloat16 [4096, 2048], P('tp'), may hold values from -2 to 2
- chosen: int32 [96, 32], P('kv'), may hold values from -1 to 95, as said below
Outputs:
- attended: bfloat16 [6144, 2048], P(('kv', 'tp'))
- log_total: float32 [6144, 16], P('kv', 'tp')
Inputs may be any that keep to these rules, and one draw needn't show every extreme that they name: `chosen`: row g names blocks at or before block g, no block twice; entry 0 is g itself; entries -1 name nothing and stand after the others. The 12 rows of one device together name exactly 2 distinct blocks of every earlier device's positions and none of a later device's.
All inputs are finite; a program needn't handle non-finite values.
Results may differ from a plain program's by a relative error of at most 0.01.
Values may be sent and summed in bfloat16 or wider, within the bound.
No kernel may reach another device: no remote copies, remote signals or barrier semaphores. Data moves between devices by JAX's collectives and lax.ppermute only.
A program may use at most 192 MiB of HBM per device.

v0:
```python
import math

import jax
import jax.numpy as jnp
from jax import lax
from jax.sharding import PartitionSpec as P

CAP = 2


epsilon = 1e-06


def latents_of(tokens, w_latent, latent_gain):
    projected = jnp.dot(tokens, w_latent, preferred_element_type=jnp.float32)
    inv_rms = lax.rsqrt(jnp.mean(projected * projected, axis=-1, keepdims=True) + epsilon)
    return (projected * inv_rms * latent_gain).astype(jnp.bfloat16)


def attend(query_part, key_rows, picked, query_blocks, blk_len, score_scale):
    group_size, picks_each = picked.shape
    offsets = jnp.arange(blk_len, dtype=jnp.int32)
    key_pos = (picked[:, :, None] * blk_len + offsets[None, None, :]).reshape(
        group_size, picks_each * blk_len
    )
    usable = jnp.repeat(picked >= 0, blk_len, axis=1)
    query_pos = query_blocks[:, None] * blk_len + offsets[None, :]
    allowed = usable[:, None, :] & (key_pos[:, None, :] <= query_pos[:, :, None])
    scores = (
        jnp.einsum("gqhr,gkr->ghqk", query_part, key_rows, preferred_element_type=jnp.float32)
        * score_scale
    )
    scores = jnp.where(allowed[:, None, :, :], scores, -jnp.inf)
    peak_score = jnp.max(scores, axis=3, keepdims=True)
    raised = jnp.exp(scores - peak_score)
    total_mass = jnp.sum(raised, axis=3)
    weights = raised.astype(jnp.bfloat16)
    summed = jnp.einsum("ghqk,gkr->gqhr", weights, key_rows, preferred_element_type=jnp.float32)
    mass_t = jnp.transpose(total_mass, (0, 2, 1))
    heads_out = (summed / mass_t[..., None]).astype(jnp.bfloat16)
    log_part = jnp.transpose(peak_score[..., 0], (0, 2, 1)) + jnp.log(mass_t)
    return (heads_out, log_part)


def slot_table(hit_mask):
    counted = jnp.cumsum(hit_mask.astype(jnp.int32), axis=1) - 1
    slot_ids = jnp.arange(CAP, dtype=jnp.int32)
    match_mask = hit_mask[:, None, :] & (counted[:, None, :] == slot_ids[None, :, None])
    places = jnp.arange(hit_mask.shape[1], dtype=jnp.int32)
    found = jnp.sum(jnp.where(match_mask, places[None, None, :], 0), axis=2)
    slot_list = jnp.where(jnp.any(match_mask, axis=2), found, -1)
    return (counted, slot_list)


def local(tokens, w_query, w_latent, latent_gain, w_output, chosen):
    tok_rows = tokens.shape[0]
    lat_rank = w_latent.shape[1]
    head_count = w_query.shape[1] // lat_rank
    per_device, picks_each = chosen.shape
    blk_len = tok_rows // per_device
    devices = lax.axis_size("kv")
    my_index = lax.axis_index("kv")
    latent = latents_of(tokens, w_latent, latent_gain)
    safe_ids = jnp.maximum(chosen, 0)
    own_blocks = latent.reshape(per_device, blk_len, lat_rank)
    flat_ids = chosen.reshape(per_device * picks_each)
    every_block = jnp.arange(devices * per_device, dtype=jnp.int32)
    owners = jnp.arange(devices, dtype=jnp.int32)
    others = (owners != my_index)[:, None]
    wanted = (
        jnp.any(flat_ids[:, None] == every_block[None, :], axis=0).reshape(devices, per_device)
        & others
    )
    counted, request = slot_table(wanted)
    reply_blocks = jnp.take(
        own_blocks,
        jnp.maximum(lax.all_to_all(request, "kv", split_axis=0, concat_axis=0, tiled=True), 0),
        axis=0,
    )
    fetched = lax.all_to_all(reply_blocks, "kv", split_axis=0, concat_axis=0, tiled=True)
    key_table = jnp.concatenate(
        [own_blocks, fetched.reshape(devices * CAP, blk_len, lat_rank)], axis=0
    )
    owner_of = safe_ids // per_device
    rank_of = jnp.take(counted.reshape(devices * per_device), safe_ids)
    lookup = jnp.where(
        owner_of == my_index,
        safe_ids - my_index * per_device,
        per_device + owner_of * CAP + rank_of,
    )
    queries = jnp.dot(tokens, w_query, preferred_element_type=jnp.float32).astype(jnp.bfloat16)
    queries = queries.reshape(per_device, blk_len, head_count, lat_rank)
    group_size = math.gcd(per_device, max(1, 512 // (blk_len * head_count)))
    first_block = my_index * per_device
    score_scale = lat_rank ** (-0.5)

    def one_group(offset):
        picked = lax.dynamic_slice_in_dim(chosen, offset, group_size, 0)
        located = lax.dynamic_slice_in_dim(lookup, offset, group_size, 0)
        query_part = lax.dynamic_slice_in_dim(queries, offset, group_size, 0)
        key_rows = jnp.take(key_table, located, axis=0).reshape(
            group_size, picks_each * blk_len, lat_rank
        )
        query_blocks = first_block + offset + jnp.arange(group_size, dtype=jnp.int32)
        return attend(query_part, key_rows, picked, query_blocks, blk_len, score_scale)

    group_starts = jnp.arange(0, per_device, group_size, dtype=jnp.int32)
    heads_out, log_total = lax.map(one_group, group_starts)
    heads_flat = heads_out.reshape(tok_rows, head_count * lat_rank)
    log_total = log_total.reshape(tok_rows, head_count)
    attended = lax.psum_scatter(
        jnp.dot(heads_flat, w_output, preferred_element_type=jnp.float32).astype(jnp.bfloat16),
        "tp",
        scatter_dimension=0,
        tiled=True,
    )
    return (attended, log_total)


def solution(mesh):
    placed = (P("kv", None), P(None, "tp"), P(), P(), P("tp", None), P("kv", None))
    return jax.shard_map(
        local,
        mesh=mesh,
        in_specs=placed,
        out_specs=(P(("kv", "tp"), None), P("kv", "tp")),
        check_vma=False,
    )
```

profile of v0, /device:TPU:0, one launch (start us, length us, event | category | flops | bytes accessed | tf_op | source)
XLA Modules:
  0.0 218.4 jit_solution(2294472344887354751)
XLA Ops:
  7.2 0.9 eq.36
  9.6 7.3 %all-to-all-start = ((s32[8,1,2]{2,1,0:T(1,128)}), s32[8,1,2]{2,1,0:T(1,128)S(1)}, u32[]{:S(2)}, u32[]{:S(2)}) async-start(s32[8,1,2]{2,1,0:T(1,128)} %copy.23), calls=%async_computation | async-start | bytes 8192 | tf_op jit(solution)/shard_map/all_to_all | solution.py:77
  17.7 3.1 %multiply_reduce_fusion = (f32[768]{0:T(1024)S(1)}, f32[768,256]{1,0:T(8,128)}) fusion(bf16[768,2048]{1,0:T(8,128)(2,1)S(1)} %copy-done, bf16[2048,256]{1,0:T(8,128)(2,1)} %param.10), kind=kOutput, calls=%fused_computation.37 | convolution fusion | flops 805698816 | bytes 4983808 | tf_op jit(solution)/shard_map/dot_general | solution.py:15
  20.9 2.7 %gather_fusion.1 = s32[384]{0:T(512)S(1)} fusion(s32[96]{0:T(128)S(1)} %sub.30, s32[1024]{0:T(1024)S(1)} %pad_clamp_fusion.2), kind=kCustom, calls=%fused_computation.1 | custom fusion | bytes 4608 | tf_op jit(solution)/shard_map/jit(_take)/gather | solution.py:85
  23.6 1.3 multiply_convert_fusion
  26.8 1.3 copy.24
  28.1 0.7 copy.25
  28.9 1.4 gather_fusion.2
  30.2 1.9 broadcast_select_fusion
  32.2 6.0 %all-to-all-start.1 = ((bf16[8,2,64,256]{3,2,1,0:T(8,128)(2,1)}), bf16[8,2,64,256]{3,2,1,0:T(8,128)(2,1)}, u32[]{:S(2)}, u32[]{:S(2)}) async-start(bf16[8,2,64,256]{3,2,1,0:T(8,128)(2,1)} %broadcast_select_fusion), calls=%async_computation.1 | async-start | bytes 1048576 | tf_op jit(solution)/shard_map/all_to_all | solution.py:80
  38.2 6.7 %convolution_convert_fusion.1 = bf16[768,1024]{1,0:T(8,128)(2,1)} fusion(bf16[768,2048]{1,0:T(8,128)(2,1)S(1)} %copy-done, bf16[2048,1024]{1,0:T(8,128)(2,1)} %param.9), kind=kOutput, calls=%fused_computation.34 | convolution fusion | flops 3222011904 | bytes 8912896 | tf_op jit(solution)/shard_map/dot_general | solution.py:91
  44.9 3.9 %reshape.161 = bf16[12,64,4,256]{3,2,1,0:T(4,128)(2,1)} reshape(bf16[768,1024]{1,0:T(8,128)(2,1)} %convolution_convert_fusion.1) | data formatting | bytes 3145728 | tf_op jit(solution)/shard_map/reshape | solution.py:92
  50.0 2.3 %all-to-all-done.1 = bf16[8,2,64,256]{3,2,1,0:T(8,128)(2,1)} async-done(((bf16[8,2,64,256]{3,2,1,0:T(8,128)(2,1)}), bf16[8,2,64,256]{3,2,1,0:T(8,128)(2,1)}, u32[]{:S(2)}, u32[]{:S(2)}) %all-to-all-start.1) | async-done | bytes 524320 | tf_op jit(solution)/shard_map/all_to_all | solution.py:80
  52.3 2.0 pad_maximum_fusion
  54.3 111.4 %while.12 = (s32[]{:T(128)}, bf16[6,2,64,4,256]{4,3,2,1,0:T(4,128)(2,1)}, f32[6,2,64,4]{2,1,0,3:T(2,128)}, s32[6]{0:T(128)}, s32[12,32]{1,0:T(8,128)}, /*index=5...) while((s32[]{:T(128)}, ...), condition=%wide.region_8.9_spmd, body=%wide.region_5.8_spmd.sunk | while | flops 1082922112 | bytes 35847144 | solution.py:108
  54.3 1.2 dynamic_slice.28
  57.4 0.7 compare_and_fusion.4
  58.3 3.2 %gather_fusion = bf16[64,64,256]{2,1,0:T(8,128)(2,1)} fusion(bf16[28,64,256]{2,1,0:T(8,128)(2,1)} %get-tuple-element.209, s32[1024]{0:T(1024)S(1)} %pad_clamp_fusion.4), kind=kCustom, calls=%fused_computation.clone.1 | custom fusion | bytes 4194560 | tf_op jit(solution)/shard_map/while/body/eval_jaxpr/jit(_take)/gather | solution.py:101
  61.6 2.9 %bitcast_select_fusion.3 = bf16[2,2048,256]{2,1,0:T(8,128)(2,1)} fusion(pred[2,2048]{1,0:T(4,128)(4,1)S(1)} %broadcast_in_dim.122, bf16[2,2048,256]{2,1,0:T(8,128)(2,1)} %bitcast.78), kind=kLoop, calls=%fused_computation.10.clone.1 | loop fusion | flops 1048576 | bytes 4198400 | tf_op jit(solution)/shard_map/while/body/eval_jaxpr/jit(_take)/select_n | solution.py:101
  66.0 1.0 constant_dynamic-slice_fusion.4
  67.0 2.6 %fusion.53 = (f32[2,4,64]{2,1,0:T(4,128)S(1)}, f32[2,4,64,2048]{3,2,1,0:T(8,128)S(1)}) fusion(bf16[2,64,4,256]{3,2,1,0:T(4,128)(2,1)S(1)} %constant_dynamic-slice_fusion.4, bf16[2,2048,256]{2,1,0:T(8,128)(2,1)} %bitcast_select_fusion.3, pred[2,64,2048]{2,1,0:T(8,128)(4,1)S(1)} %compare_and_fusion.5), kind=kOutput, calls=%fused_computation.62.clone.1 | convolution fusion | flops 540016128 | bytes 6817792 | tf_op jit(solution)/shard_map/while/body/eval_jaxpr/gqhr,gkr->ghqk/dot_general | solution.py:30
  71.2 0.8 fusion.55
  71.9 0.9 copy_dynamic-update-slice_fusion.4
  72.9 1.2 dynamic_slice.28
  76.0 0.7 compare_and_fusion.4
  76.8 3.2 %gather_fusion = bf16[64,64,256]{2,1,0:T(8,128)(2,1)} fusion(bf16[28,64,256]{2,1,0:T(8,128)(2,1)} %get-tuple-element.209, s32[1024]{0:T(1024)S(1)} %pad_clamp_fusion.4), kind=kCustom, calls=%fused_computation.clone.1 | custom fusion | bytes 4194560 | tf_op jit(solution)/shard_map/while/body/eval_jaxpr/jit(_take)/gather | solution.py:101
  80.2 2.9 %bitcast_select_fusion.3 = bf16[2,2048,256]{2,1,0:T(8,128)(2,1)} fusion(pred[2,2048]{1,0:T(4,128)(4,1)S(1)} %broadcast_in_dim.122, bf16[2,2048,256]{2,1,0:T(8,128)(2,1)} %bitcast.78), kind=kLoop, calls=%fused_computation.10.clone.1 | loop fusion | flops 1048576 | bytes 4198400 | tf_op jit(solution)/shard_map/while/body/eval_jaxpr/jit(_take)/select_n | solution.py:101
  84.5 1.0 constant_dynamic-slice_fusion.4
  85.6 2.6 %fusion.53 = (f32[2,4,64]{2,1,0:T(4,128)S(1)}, f32[2,4,64,2048]{3,2,1,0:T(8,128)S(1)}) fusion(bf16[2,64,4,256]{3,2,1,0:T(4,128)(2,1)S(1)} %constant_dynamic-slice_fusion.4, bf16[2,2048,256]{2,1,0:T(8,128)(2,1)} %bitcast_select_fusion.3, pred[2,64,2048]{2,1,0:T(8,128)(4,1)S(1)} %compare_and_fusion.5), kind=kOutput, calls=%fused_computation.62.clone.1 | convolution fusion | flops 540016128 | bytes 6817792 | tf_op jit(solution)/shard_map/while/body/eval_jaxpr/gqhr,gkr->ghqk/dot_general | solution.py:30
  89.7 0.8 fusion.55
  90.5 0.9 copy_dynamic-update-slice_fusion.4
  91.4 1.2 dynamic_slice.28
  94.6 0.7 compare_and_fusion.4
  95.4 3.2 %gather_fusion = bf16[64,64,256]{2,1,0:T(8,128)(2,1)} fusion(bf16[28,64,256]{2,1,0:T(8,128)(2,1)} %get-tuple-element.209, s32[1024]{0:T(1024)S(1)} %pad_clamp_fusion.4), kind=kCustom, calls=%fused_computation.clone.1 | custom fusion | bytes 4194560 | tf_op jit(solution)/shard_map/while/body/eval_jaxpr/jit(_take)/gather | solution.py:101
  98.7 2.9 %bitcast_select_fusion.3 = bf16[2,2048,256]{2,1,0:T(8,128)(2,1)} fusion(pred[2,2048]{1,0:T(4,128)(4,1)S(1)} %broadcast_in_dim.122, bf16[2,2048,256]{2,1,0:T(8,128)(2,1)} %bitcast.78), kind=kLoop, calls=%fused_computation.10.clone.1 | loop fusion | flops 1048576 | bytes 4198400 | tf_op jit(solution)/shard_map/while/body/eval_jaxpr/jit(_take)/select_n | solution.py:101
  103.1 1.0 constant_dynamic-slice_fusion.4
  104.2 2.6 %fusion.53 = (f32[2,4,64]{2,1,0:T(4,128)S(1)}, f32[2,4,64,2048]{3,2,1,0:T(8,128)S(1)}) fusion(bf16[2,64,4,256]{3,2,1,0:T(4,128)(2,1)S(1)} %constant_dynamic-slice_fusion.4, bf16[2,2048,256]{2,1,0:T(8,128)(2,1)} %bitcast_select_fusion.3, pred[2,64,2048]{2,1,0:T(8,128)(4,1)S(1)} %compare_and_fusion.5), kind=kOutput, calls=%fused_computation.62.clone.1 | convolution fusion | flops 540016128 | bytes 6817792 | tf_op jit(solution)/shard_map/while/body/eval_jaxpr/gqhr,gkr->ghqk/dot_general | solution.py:30
  108.3 0.8 fusion.55
  109.1 0.9 copy_dynamic-update-slice_fusion.4
  110.0 1.2 dynamic_slice.28
  113.1 0.7 compare_and_fusion.4
  114.0 3.2 %gather_fusion = bf16[64,64,256]{2,1,0:T(8,128)(2,1)} fusion(bf16[28,64,256]{2,1,0:T(8,128)(2,1)} %get-tuple-element.209, s32[1024]{0:T(1024)S(1)} %pad_clamp_fusion.4), kind=kCustom, calls=%fused_computation.clone.1 | custom fusion | bytes 4194560 | tf_op jit(solution)/shard_map/while/body/eval_jaxpr/jit(_take)/gather | solution.py:101
  117.3 2.9 %bitcast_select_fusion.3 = bf16[2,2048,256]{2,1,0:T(8,128)(2,1)} fusion(pred[2,2048]{1,0:T(4,128)(4,1)S(1)} %broadcast_in_dim.122, bf16[2,2048,256]{2,1,0:T(8,128)(2,1)} %bitcast.78), kind=kLoop, calls=%fused_computation.10.clone.1 | loop fusion | flops 1048576 | bytes 4198400 | tf_op jit(solution)/shard_map/while/body/eval_jaxpr/jit(_take)/select_n | solution.py:101
  121.7 1.0 constant_dynamic-slice_fusion.4
  122.7 2.6 %fusion.53 = (f32[2,4,64]{2,1,0:T(4,128)S(1)}, f32[2,4,64,2048]{3,2,1,0:T(8,128)S(1)}) fusion(bf16[2,64,4,256]{3,2,1,0:T(4,128)(2,1)S(1)} %constant_dynamic-slice_fusion.4, bf16[2,2048,256]{2,1,0:T(8,128)(2,1)} %bitcast_select_fusion.3, pred[2,64,2048]{2,1,0:T(8,128)(4,1)S(1)} %compare_and_fusion.5), kind=kOutput, calls=%fused_computation.62.clone.1 | convolution fusion | flops 540016128 | bytes 6817792 | tf_op jit(solution)/shard_map/while/body/eval_jaxpr/gqhr,gkr->ghqk/dot_general | solution.py:30
  126.9 0.8 fusion.55
  127.6 0.9 copy_dynamic-update-slice_fusion.4
  128.6 1.2 dynamic_slice.28
  132.5 3.2 %gather_fusion = bf16[64,64,256]{2,1,0:T(8,128)(2,1)} fusion(bf16[28,64,256]{2,1,0:T(8,128)(2,1)} %get-tuple-element.209, s32[1024]{0:T(1024)S(1)} %pad_clamp_fusion.4), kind=kCustom, calls=%fused_computation.clone.1 | custom fusion | bytes 4194560 | tf_op jit(solution)/shard_map/while/body/eval_jaxpr/jit(_take)/gather | solution.py:101
  135.8 2.9 %bitcast_select_fusion.3 = bf16[2,2048,256]{2,1,0:T(8,128)(2,1)} fusion(pred[2,2048]{1,0:T(4,128)(4,1)S(1)} %broadcast_in_dim.122, bf16[2,2048,256]{2,1,0:T(8,128)(2,1)} %bitcast.78), kind=kLoop, calls=%fused_computation.10.clone.1 | loop fusion | flops 1048576 | bytes 4198400 | tf_op jit(solution)/shard_map/while/body/eval_jaxpr/jit(_take)/select_n | solution.py:101
  140.2 1.0 constant_dynamic-slice_fusion.4
  141.3 2.6 %fusion.53 = (f32[2,4,64]{2,1,0:T(4,128)S(1)}, f32[2,4,64,2048]{3,2,1,0:T(8,128)S(1)}) fusion(bf16[2,64,4,256]{3,2,1,0:T(4,128)(2,1)S(1)} %constant_dynamic-slice_fusion.4, bf16[2,2048,256]{2,1,0:T(8,128)(2,1)} %bitcast_select_fusion.3, pred[2,64,2048]{2,1,0:T(8,128)(4,1)S(1)} %compare_and_fusion.5), kind=kOutput, calls=%fused_computation.62.clone.1 | convolution fusion | flops 540016128 | bytes 6817792 | tf_op jit(solution)/shard_map/while/body/eval_jaxpr/gqhr,gkr->ghqk/dot_general | solution.py:30
  145.4 0.8 fusion.55
  146.2 0.9 copy_dynamic-update-slice_fusion.4
  147.1 1.2 dynamic_slice.28
  151.1 3.2 %gather_fusion = bf16[64,64,256]{2,1,0:T(8,128)(2,1)} fusion(bf16[28,64,256]{2,1,0:T(8,128)(2,1)} %get-tuple-element.209, s32[1024]{0:T(1024)S(1)} %pad_clamp_fusion.4), kind=kCustom, calls=%fused_computation.clone.1 | custom fusion | bytes 4194560 | tf_op jit(solution)/shard_map/while/body/eval_jaxpr/jit(_take)/gather | solution.py:101
  154.4 2.9 %bitcast_select_fusion.3 = bf16[2,2048,256]{2,1,0:T(8,128)(2,1)} fusion(pred[2,2048]{1,0:T(4,128)(4,1)S(1)} %broadcast_in_dim.122, bf16[2,2048,256]{2,1,0:T(8,128)(2,1)} %bitcast.78), kind=kLoop, calls=%fused_computation.10.clone.1 | loop fusion | flops 1048576 | bytes 4198400 | tf_op jit(solution)/shard_map/while/body/eval_jaxpr/jit(_take)/select_n | solution.py:101
  158.8 1.0 constant_dynamic-slice_fusion.4
  159.8 2.6 %fusion.53 = (f32[2,4,64]{2,1,0:T(4,128)S(1)}, f32[2,4,64,2048]{3,2,1,0:T(8,128)S(1)}) fusion(bf16[2,64,4,256]{3,2,1,0:T(4,128)(2,1)S(1)} %constant_dynamic-slice_fusion.4, bf16[2,2048,256]{2,1,0:T(8,128)(2,1)} %bitcast_select_fusion.3, pred[2,64,2048]{2,1,0:T(8,128)(4,1)S(1)} %compare_and_fusion.5), kind=kOutput, calls=%fused_computation.62.clone.1 | convolution fusion | flops 540016128 | bytes 6817792 | tf_op jit(solution)/shard_map/while/body/eval_jaxpr/gqhr,gkr->ghqk/dot_general | solution.py:30
  164.0 0.8 fusion.55
  164.8 0.9 copy_dynamic-update-slice_fusion.4
  165.7 1.8 copy.36
  167.5 7.0 %convolution_convert_fusion = bf16[768,2048]{1,0:T(8,128)(2,1)} fusion(bf16[768,1024]{1,0:T(8,128)(2,1)S(1)} %bitcast.82, bf16[1024,2048]{1,0:T(8,128)(2,1)} %param.12), kind=kOutput, calls=%fused_computation.33 | convolution fusion | flops 3222798336 | bytes 8912896 | tf_op jit(solution)/shard_map/dot_general | solution.py:112
  175.8 35.7 %reduce-scatter.2.cloned.1.call-done = bf16[192,2048]{1,0:T(8,128)(2,1)} async-done(((bf16[768,2048]{1,0:T(8,128)(2,1)}), bf16[192,2048]{1,0:T(8,128)(2,1)}) %reduce-scatter.2.cloned.1.call-update) | async-done | bytes 786448 | tf_op jit(solution)/shard_map/reduce_scatter | solution.py:111
  (156 shorter events, 23.9 us)
Async XLA Ops:
  7.2 10.5 %copy-start = (bf16[768,2048]{1,0:T(8,128)(2,1)S(1)}, bf16[768,2048]{1,0:T(8,128)(2,1)}, u32[]{:S(2)}) copy-start(bf16[768,2048]{1,0:T(8,128)(2,1)} %param.8) | copy-start | bytes 9437188
  9.6 15.4 %all-to-all-start = ((s32[8,1,2]{2,1,0:T(1,128)}), s32[8,1,2]{2,1,0:T(1,128)S(1)}, u32[]{:S(2)}, u32[]{:S(2)}) async-start(s32[8,1,2]{2,1,0:T(1,128)} %copy.23), calls=%async_computation | async-start | bytes 8192 | tf_op jit(solution)/shard_map/all_to_all | solution.py:77
  32.2 20.1 %all-to-all-start.1 = ((bf16[8,2,64,256]{3,2,1,0:T(8,128)(2,1)}), bf16[8,2,64,256]{3,2,1,0:T(8,128)(2,1)}, u32[]{:S(2)}, u32[]{:S(2)}) async-start(bf16[8,2,64,256]{3,2,1,0:T(8,128)(2,1)} %broadcast_select_fusion), calls=%async_computation.1 | async-start | bytes 1048576 | tf_op jit(solution)/shard_map/all_to_all | solution.py:80
  38.2 173.3 %reduce-scatter.2.cloned.1.call-start = ((), (), s32[]{:S(2)}) async-start(), calls=%async_computation.3 | async-start | bytes 3932160 | tf_op jit(solution)/shard_map/reduce_scatter | solution.py:111
  44.9 4.4 %copy-start.2 = (s32[12,32]{1,0:T(8,128)S(1)}, s32[12,32]{1,0:T(8,128)}, u32[]{:S(2)}) copy-start(s32[12,32]{1,0:T(8,128)} %param.13) | copy-start | bytes 4612
  69.6 1.6 copy-start.1
  88.1 1.6 copy-start.1
  106.7 1.6 copy-start.1
  125.3 1.6 copy-start.1
  143.8 1.6 copy-start.1
  162.4 1.6 copy-start.1
  174.4 0.7 copy-start.3
Sparse Core Ops, SparseCore 0:
  174.6 36.9 reduce-scatter.1
where the time goes:
time: 221 us; the launch traced here: 218 us
  local copies, waits for them, and re-layouts  62.8 us (28%)
  waiting for transfers between devices  38 us (17%)
  other arithmetic  37.4 us (17%)
  matrix products  36.7 us (17%)
  loops' own time  16 us (7%)
  between operations  14.1 us (6%)
  starting transfers between devices  13.3 us (6%)
    reduce_scatter x1, waiting for transfers between devices, local(): lax.psum_scatter(jnp.dot(heads_flat, w_output, preferred_element_type=jnp...  35.7 us
    gather x6, local copies, waits for them, and re-layouts, one_group(): jnp.take(key_table, located, axis=0)  18.9 us
    select_n x6, other arithmetic, one_group(): jnp.take(key_table, located, axis=0)  17.6 us
    another operation x1, loops' own time, local(): heads_out, log_total = lax.map(one_group, group_starts)  16 us
    dot_general x6, matrix products, attend(): jnp.einsum('gqhr,gkr->ghqk', query_part, key_rows, preferred_element_type...  15.4 us
    dynamic_update_slice x12, local copies, waits for them, and re-layouts, local(): heads_out, log_total = lax.map(one_group, group_starts)  9.13 us
    all_to_all x1, starting transfers between devices, local(): lax.all_to_all(request, 'kv', split_axis=0, concat_axis=0, tiled=True)  7.31 us
    dynamic_slice x6, local copies, waits for them, and re-layouts, local(): heads_out, log_total = lax.map(one_group, group_starts)  7.2 us
  transfers between devices with their start and end apart: 3, of which 2 were waited for; matrix products, arithmetic and copies ran while one was open for 9% of the time, Pallas kernels for 0%

commit v1 on v0

v1 whole, which is shorter than its diff:
```python
import functools
import math

import jax
import jax.numpy as jnp
from jax import lax
from jax.experimental import pallas as pl
from jax.experimental.pallas import tpu as pltpu
from jax.sharding import PartitionSpec as P

CAP = 2
NEG = -1e30
epsilon = 1e-06
VMEM = pltpu.VMEM


def latent_kernel(tok_ref, w_ref, gain_ref, out_ref):
    projected = jnp.dot(tok_ref[...], w_ref[...], preferred_element_type=jnp.float32)
    inv_rms = lax.rsqrt(jnp.mean(projected * projected, axis=-1, keepdims=True) + epsilon)
    out_ref[...] = (projected * inv_rms * gain_ref[...]).astype(out_ref.dtype)


def latents_of(tokens, w_latent, latent_gain):
    rows, width = tokens.shape
    rank = w_latent.shape[1]
    tile = math.gcd(rows, 256)
    return pl.pallas_call(
        latent_kernel,
        grid=(rows // tile,),
        in_specs=[
            pl.BlockSpec((tile, width), lambda i: (i, 0)),
            pl.BlockSpec((width, rank), lambda i: (0, 0)),
            pl.BlockSpec((1, rank), lambda i: (0, 0)),
        ],
        out_specs=pl.BlockSpec((tile, rank), lambda i: (i, 0)),
        out_shape=jax.ShapeDtypeStruct((rows, rank), jnp.bfloat16),
        cost_estimate=pl.CostEstimate(
            flops=2 * rows * width * rank, bytes_accessed=2 * rows * width, transcendentals=rows
        ),
        name="latents",
    )(tokens, w_latent, latent_gain.reshape(1, rank))


def query_kernel(core_ref, tok_ref, w_ref, out_ref):
    m, _, tile, width = tok_ref.shape
    rows = tok_ref[...].reshape(m * tile, width)
    out = jnp.dot(rows, w_ref[...], preferred_element_type=jnp.float32)
    out_ref[...] = out.astype(out_ref.dtype)


def queries_of(core, tokens4, w_query, rank):
    m, pair, tile, width = tokens4.shape
    cols = w_query.shape[1]
    return pl.pallas_call(
        query_kernel,
        grid_spec=pltpu.PrefetchScalarGridSpec(
            num_scalar_prefetch=1,
            grid=(cols // rank,),
            in_specs=[
                pl.BlockSpec((m, 1, tile, width), lambda i, core: (0, core[0], 0, 0)),
                pl.BlockSpec((width, rank), lambda i, core: (0, i)),
            ],
            out_specs=pl.BlockSpec((m * tile, rank), lambda i, core: (0, i)),
        ),
        out_shape=jax.ShapeDtypeStruct((m * tile, cols), jnp.bfloat16),
        cost_estimate=pl.CostEstimate(
            flops=2 * m * tile * width * cols,
            bytes_accessed=2 * width * cols,
            transcendentals=0,
        ),
        name="queries",
    )(core, tokens4, w_query)


def pick_kernel(meta_ref, lat_ref, out_ref):
    for i in range(out_ref.shape[0]):
        out_ref[i] = lat_ref[meta_ref[i], meta_ref[out_ref.shape[0]]]


def pick_halves(meta, latent4, count):
    _, _, half, rank = latent4.shape
    return pl.pallas_call(
        pick_kernel,
        grid_spec=pltpu.PrefetchScalarGridSpec(
            num_scalar_prefetch=1,
            in_specs=[pl.BlockSpec(memory_space=VMEM)],
            out_specs=pl.BlockSpec(memory_space=VMEM),
        ),
        out_shape=jax.ShapeDtypeStruct((count, half, rank), latent4.dtype),
        name="pick",
    )(meta, latent4)


def attend_kernel(
    scale, meta_ref, qa_ref, qb_ref, own_ref, r1_ref, r2_ref, bias_ref, ho_ref, lse_ref, s_ref, p_ref, bl_ref
):
    blk_len = qa_ref.shape[2]
    rank = own_ref.shape[1]
    heads = qa_ref.shape[3] // rank
    own_len = own_ref.shape[0]
    rem_len = r1_ref.shape[0]
    key_len = own_len + 2 * rem_len
    unit = heads * blk_len
    exp_scale = scale * math.log2(math.e)
    row0 = (meta_ref[1] + pl.program_id(0)) * blk_len
    k_pos = lax.broadcasted_iota(jnp.int32, (blk_len, own_len), 1)
    q_pos = lax.broadcasted_iota(jnp.int32, (blk_len, own_len), 0) + row0
    bl_ref[...] = jnp.where(k_pos <= q_pos, bias_ref[0, :, :own_len], NEG)
    tile = math.gcd(math.gcd(own_len, rem_len), 256)
    parts = []
    base = 0
    for ref in (own_ref, r1_ref, r2_ref):
        for at in range(0, ref.shape[0], tile):
            parts.append((ref, at, base + at))
        base += ref.shape[0]
    for u, q_ref in enumerate((qa_ref, qb_ref)):
        q = jnp.concatenate(
            [q_ref[0, 0, :, h * rank : (h + 1) * rank] for h in range(heads)], axis=0
        )
        for ref, at, col in parts:
            s = lax.dot_general(
                q, ref[at : at + tile, :], (((1,), (1,)), ((), ())), preferred_element_type=jnp.float32
            )
            if col < own_len:
                add = bl_ref[:, col : col + tile][None]
            else:
                add = bias_ref[0, :, col : col + tile][None]
            s = s.reshape(heads, blk_len, tile) + add
            s_ref[u * unit : (u + 1) * unit, col : col + tile] = s.reshape(unit, tile)
    lses = []
    for u in range(2):
        masses = []
        for h in range(heads):
            at = u * unit + h * blk_len
            peak = s_ref[at : at + blk_len, 0:128]
            for col in range(128, key_len, 128):
                peak = jnp.maximum(peak, s_ref[at : at + blk_len, col : col + 128])
            peak = jnp.max(peak, axis=1, keepdims=True)
            mass = jnp.zeros((blk_len, 128), jnp.float32)
            for col in range(0, key_len, 128):
                raised = jnp.exp2((s_ref[at : at + blk_len, col : col + 128] - peak) * exp_scale)
                mass = mass + raised
                p_ref[at : at + blk_len, col : col + 128] = raised.astype(p_ref.dtype)
            mass = jnp.sum(mass, axis=1, keepdims=True)
            masses.append(1.0 / mass)
            lses.append(peak * scale + jnp.log(mass))
        out = jnp.zeros((unit, rank), jnp.float32)
        base = 0
        for ref in (own_ref, r1_ref, r2_ref):
            n = ref.shape[0]
            out = out + jnp.dot(
                p_ref[u * unit : (u + 1) * unit, base : base + n], ref[...], preferred_element_type=jnp.float32
            )
            base += n
        for h in range(heads):
            ho_ref[0, :, (u * heads + h) * rank : (u * heads + h + 1) * rank] = (
                out[h * blk_len : (h + 1) * blk_len] * masses[h]
            ).astype(ho_ref.dtype)
    lse_ref[0] = jnp.concatenate(lses, axis=1)


def attend(meta, qa, qb, latent, r1, r2, bias, first, count, scale):
    _, _, blk_len, cols = qa.shape
    rank = latent.shape[1]
    heads = 2 * cols // rank
    key_len = bias.shape[-1]
    q_spec = pl.BlockSpec((1, 1, blk_len, cols), lambda i, meta: (meta[0], first + i, 0, 0))

    def whole(array):
        return pl.BlockSpec(array.shape, lambda i, meta: (0, 0))

    rows = heads * blk_len
    return pl.pallas_call(
        functools.partial(attend_kernel, scale),
        grid_spec=pltpu.PrefetchScalarGridSpec(
            num_scalar_prefetch=1,
            grid=(count,),
            in_specs=[
                q_spec,
                q_spec,
                whole(latent),
                whole(r1),
                whole(r2),
                pl.BlockSpec((1, 1, key_len), lambda i, meta: (meta[1] + i, 0, 0)),
            ],
            out_specs=[
                pl.BlockSpec((1, blk_len, 2 * cols), lambda i, meta: (i, 0, 0)),
                pl.BlockSpec((1, blk_len, heads), lambda i, meta: (i, 0, 0)),
            ],
            scratch_shapes=[
                VMEM((rows, key_len), jnp.float32),
                VMEM((rows, key_len), jnp.bfloat16),
                VMEM((blk_len, latent.shape[0]), jnp.float32),
            ],
        ),
        out_shape=[
            jax.ShapeDtypeStruct((count, blk_len, 2 * cols), jnp.bfloat16),
            jax.ShapeDtypeStruct((count, blk_len, heads), jnp.float32),
        ],
        cost_estimate=pl.CostEstimate(
            flops=4 * count * rows * key_len * rank,
            bytes_accessed=2 * key_len * rank,
            transcendentals=count * rows * key_len,
        ),
        name="attend",
    )(meta, qa, qb, latent, r1, r2, bias)


def local(tokens, w_query, w_latent, latent_gain, w_output, chosen):
    tok_rows, width = tokens.shape
    rank = w_latent.shape[1]
    heads = w_query.shape[1] // rank
    per_device, picks = chosen.shape
    blk_len = tok_rows // per_device
    half = blk_len // 2
    devices = lax.axis_size("kv")
    n_tp = lax.axis_size("tp")
    m = n_tp // 2
    tile_rows = tok_rows // n_tp
    tile_blocks = tile_rows // blk_len
    mine = lax.axis_index("kv")
    tp = lax.axis_index("tp")
    chip, core = tp // 2, tp % 2
    swap = [(i, i ^ 1) for i in range(n_tp)]

    wq_other = lax.ppermute(w_query, "tp", swap)
    wo_other = lax.ppermute(w_output, "tp", swap)

    flat = chosen.reshape(1, per_device * picks)
    first_id = (jnp.arange(devices, dtype=jnp.int32) * per_device)[:, None]
    of_owner = (flat >= first_id) & (flat < first_id + per_device)
    low = jnp.min(jnp.where(of_owner, flat, devices * per_device), axis=1)
    high = jnp.max(jnp.where(of_owner, flat, -1), axis=1)
    request = jnp.stack([low, high], axis=1)
    asked = lax.all_to_all(request, "kv", split_axis=0, concat_axis=0, tiled=True)

    latent = latents_of(tokens, w_latent, latent_gain)
    tokens4 = tokens.reshape(m, 2, tile_rows, width)
    core1 = core.reshape(1).astype(jnp.int32)
    qa = queries_of(core1, tokens4, w_query, rank)

    local_ids = jnp.clip(asked - mine * per_device, 0, per_device - 1).reshape(devices * CAP)
    pick_meta = jnp.concatenate([local_ids, core1])
    reply = pick_halves(pick_meta, latent.reshape(per_device, 2, half, rank), devices * CAP)
    fetched = lax.all_to_all(
        reply.reshape(devices, CAP, half, rank), "kv", split_axis=0, concat_axis=0, tiled=True
    )
    r1 = fetched.reshape(devices * CAP * half, rank)
    r2 = lax.ppermute(r1, "tp", swap)
    qb = queries_of(core1, tokens4, wq_other, rank)

    earlier = jnp.arange(devices, dtype=jnp.int32) < mine
    slots = jnp.stack(
        [jnp.where(earlier, low, -2), jnp.where(earlier & (high > low), high, -2)], axis=1
    ).reshape(devices * CAP)
    own_ids = mine * per_device + jnp.arange(per_device, dtype=jnp.int32)
    slot_keys = jnp.repeat(slots, half)
    key_ids = jnp.concatenate([jnp.repeat(own_ids, blk_len), slot_keys, slot_keys])
    named = jnp.any(chosen[:, :, None] == key_ids[None, None, :], axis=1)
    bias = jnp.where(named, 0.0, NEG).astype(jnp.float32)[:, None, :]

    qa4 = qa.reshape(m, tile_blocks, blk_len, heads * rank)
    qb4 = qb.reshape(m, tile_blocks, blk_len, heads * rank)
    scale = rank ** (-0.5)

    def work(k, first, count):
        chip_k = (chip + k) % m
        meta = jnp.stack([chip_k, (chip_k * 2 + core) * tile_blocks + first]).astype(jnp.int32)
        ho, lse = attend(meta, qa4, qb4, latent, r1, r2, bias, first, count, scale)
        ho = ho.reshape(count * blk_len, 2 * heads * rank)
        out = jnp.dot(ho[:, : heads * rank], w_output, preferred_element_type=jnp.float32)
        out = out + jnp.dot(ho[:, heads * rank :], wo_other, preferred_element_type=jnp.float32)
        return out, lse.reshape(count * blk_len, 2 * heads)

    splits = [(0, 1), (1, tile_blocks - 1)] if tile_blocks > 1 else [(0, 1)]
    lse_tiles = [None] * m
    arrived = []
    for k in range(1, m):
        to_chip = [(i, (i + 2 * k) % n_tp) for i in range(n_tp)]
        pieces, lses = [], []
        for first, count in splits:
            out, lse = work(k, first, count)
            pieces.append(lax.ppermute(out.astype(jnp.bfloat16), "tp", to_chip))
            lses.append(lse)
        arrived.append(pieces)
        lse_tiles[k] = jnp.concatenate(lses, axis=0)
    total, lse_tiles[0] = work(0, 0, tile_blocks)
    received = [jnp.concatenate(pieces, axis=0).astype(jnp.float32) for pieces in arrived]
    for piece in received:
        total = total + piece
    attended = total.astype(jnp.bfloat16)

    lse = jnp.stack(lse_tiles)
    lse = lax.dynamic_slice_in_dim(jnp.concatenate([lse, lse], axis=0), (m - chip) % m, m, 0)
    theirs = lax.ppermute(lse[..., heads:], "tp", swap)
    ours = lse[..., :heads]
    log_total = jnp.where(
        core == 0, jnp.stack([ours, theirs], axis=1), jnp.stack([theirs, ours], axis=1)
    ).reshape(tok_rows, heads)
    return (attended, log_total)


def solution(mesh):
    placed = (P("kv", None), P(None, "tp"), P(), P(), P("tp", None), P("kv", None))
    return jax.shard_map(
        local,
        mesh=mesh,
        in_specs=placed,
        out_specs=(P(("kv", "tp"), None), P("kv", "tp")),
        check_vma=False,
    )
```

time: 221 us -> 92.7 us (0.42)
  local copies, waits for them, and re-layouts: 62.8 us -> 6.77 us
  Pallas kernels: 0 us -> 38.3 us
  other arithmetic: 37.4 us -> 2.92 us
  waiting for transfers between devices: 38 us -> 11.7 us
  matrix products: 36.7 us -> 15.3 us
  loops' own time: 16 us -> 0 us
  between operations: 14.1 us -> 0.87 us
  starting transfers between devices: 13.3 us -> 16 us
    pallas_call x0 -> x7, Pallas kernels: none -> 38.3 us  [the longest x3 20.1 us: attend(): pl.pallas_call(functools.partial(attend_kernel, scale), grid_spec=pltpu.P...]
    reduce_scatter x1 -> x0, waiting for transfers between devices: 35.7 us -> none  [local(): lax.psum_scatter(jnp.dot(heads_flat, w_output, preferred_element_type=jnp...]
    gather x9 -> x0, local copies, waits for them, and re-layouts: 23 us -> none  [the longest x6 18.9 us: one_group(): jnp.take(key_table, located, axis=0)]
    dot_general x15 -> x6, matrix products: 36.7 us -> 15.3 us  [the longest x3 9.51 us: work(): jnp.dot(ho[:, heads * rank:], wo_other, preferred_element_type=jnp.float32)]
    select_n x9 -> x3, other arithmetic: 20.2 us -> 0.03 us  [the longest x1 0.01 us: local(): bias = jnp.where(named, 0.0, NEG).astype(jnp.float32)[:, None, :]]
    another operation x1 -> x0, loops' own time: 16 us -> none  [local(): heads_out, log_total = lax.map(one_group, group_starts)]
    dynamic_slice x12 -> x0, local copies, waits for them, and re-layouts: 13.5 us -> none  [the longest x6 7.2 us: local(): heads_out, log_total = lax.map(one_group, group_starts)]
    ppermute x0 -> x6, waiting for transfers between devices: none -> 9.48 us  [the longest x2 9.47 us: local(): pieces.append(lax.ppermute(out.astype(jnp.bfloat16), 'tp', to_chip))]
  transfers between devices with their start and end apart: 3 -> 8, of which waited for: 2 -> 3; matrix products, arithmetic and copies ran while one was open for 9% -> 22% of each run, Pallas kernels for 0% -> 42%
where the time goes in v1:
time: 92.7 us; the launch traced here: 91.8 us
  Pallas kernels  38.3 us (41%)
  starting transfers between devices  16 us (17%)
  matrix products  15.3 us (17%)
  waiting for transfers between devices  11.7 us (13%)
  local copies, waits for them, and re-layouts  6.77 us (7%)
  other arithmetic  2.92 us (3%)
    pallas_call x3, Pallas kernels, attend(): pl.pallas_call(functools.partial(attend_kernel, scale), grid_spec=pltpu.P...  20.1 us
    pallas_call x2, Pallas kernels, queries_of(): pl.pallas_call(query_kernel, grid_spec=pltpu.PrefetchScalarGridSpec(num_s...  11.2 us
    dot_general x3, matrix products, work(): jnp.dot(ho[:, heads * rank:], wo_other, preferred_element_type=jnp.float32)  9.51 us
    ppermute x2, waiting for transfers between devices, local(): pieces.append(lax.ppermute(out.astype(jnp.bfloat16), 'tp', to_chip))  9.47 us
    all_to_all x1, starting transfers between devices, local(): lax.all_to_all(request, 'kv', split_axis=0, concat_axis=0, tiled=True)  7.25 us
    dot_general x3, matrix products, work(): jnp.dot(ho[:, :heads * rank], w_output, preferred_element_type=jnp.float32)  5.79 us
    all_to_all x1, starting transfers between devices, local(): lax.all_to_all(reply.reshape(devices, CAP, half, rank), 'kv', split_axis=...  5.34 us
    pallas_call x1, Pallas kernels, latents_of(): pl.pallas_call(latent_kernel, grid=(rows // tile,), in_specs=[pl.BlockSpe...  4.55 us
  transfers between devices with their start and end apart: 8, of which 3 were waited for; matrix products, arithmetic and copies ran while one was open for 22% of the time, Pallas kernels for 42%

profile of v1, /device:TPU:0, one launch (start us, length us, event | category | flops | bytes accessed | tf_op | source)
XLA Modules:
  0.0 91.8 jit_solution(8170164903395962127)
XLA Ops:
  0.6 0.0 copy-start.5
  0.6 0.6 collective-permute-start
  1.2 0.1 collective-permute-start.2
  1.3 0.8 ge.15
  2.1 0.2 select_reduce_fusion.1
  2.3 0.7 copy.35
  3.0 7.2 %all-to-all-start = ((s32[8,1,2]{2,1,0:T(1,128)}), s32[8,1,2]{2,1,0:T(1,128)S(1)}, u32[]{:S(2)}, u32[]{:S(2)}) async-start(s32[8,1,2]{2,1,0:T(1,128)} %copy.35), calls=%async_computation | async-start | bytes 8192 | tf_op jit(solution)/shard_map/all_to_all | solution.py:235
  10.2 0.1 copy.36
  10.3 0.1 reshape.129
  10.4 0.1 broadcast_in_dim.43
  10.5 0.1 reshape.130
  10.6 0.1 broadcast_in_dim.41
  10.6 0.1 reshape.128
  10.7 4.5 %latents.1.own_ref = bf16[768,256]{1,0:T(8,128)(2,1)} custom-call(bf16[768,2048]{1,0:T(8,128)(2,1)} %tok_ref.1, bf16[2048,256]{1,0:T(8,128)(2,1)} %w_ref.3, f32[1,256]{1,0:T(1,128)} %bitcast.71), custom_call_target="tpu_custom_call" | custom-call | flops 805306368 | bytes 3145728 | tf_op jit(solution)/shard_map/latents/pallas_call | solution.py:27
  15.3 0.0 copy-done.5
  15.3 0.7 compare_reduce_fusion
  16.0 0.7 all-to-all-done
  16.7 0.1 min.12
  16.7 0.6 pad_add_fusion.3.meta_ref
  17.3 2.4 %pick.1 = bf16[16,32,256]{2,1,0:T(8,128)(2,1)} custom-call(s32[17]{0:T(128)} %pad_add_fusion.3.meta_ref, bf16[12,2,32,256]{3,2,1,0:T(8,128)(2,1)} %bitcast.47), custom_call_target="tpu_custom_call" | custom-call | tf_op jit(solution)/shard_map/pick/pallas_call | solution.py:82
  19.7 5.3 %all-to-all-start.1 = ((bf16[8,2,32,256]{3,2,1,0:T(8,128)(2,1)}), bf16[8,2,32,256]{3,2,1,0:T(8,128)(2,1)S(1)}, u32[]{:S(2)}, u32[]{:S(2)}) async-start(bf16[8,2,32,256]{3,2,1,0:T(8,128)(2,1)} %bitcast.48), calls=%async_computation.1 | async-start | bytes 524288 | tf_op jit(solution)/shard_map/all_to_all | solution.py:245
  25.2 0.7 select_n.90.bias_ref
  25.9 0.7 pad_add_fusion.2
  26.5 5.6 %queries.2 = bf16[384,1024]{1,0:T(8,128)(2,1)} custom-call(s32[1]{0:T(128)} %bitcast.2.core_ref, bf16[2,2,192,2048]{3,2,1,0:T(8,128)(2,1)} %bitcast.45, bf16[2048,1024]{1,0:T(8,128)(2,1)} %w_ref.2), custom_call_target="tpu_custom_call" | custom-call | flops 1610612736 | bytes 4194304 | tf_op jit(solution)/shard_map/queries/pallas_call | solution.py:54
  32.1 1.6 %all-to-all-done.1 = bf16[8,2,32,256]{3,2,1,0:T(8,128)(2,1)S(1)} async-done(((bf16[8,2,32,256]{3,2,1,0:T(8,128)(2,1)}), bf16[8,2,32,256]{3,2,1,0:T(8,128)(2,1)S(1)}, u32[]{:S(2)}, u32[]{:S(2)}) %all-to-all-start.1) | async-done | bytes 262176 | tf_op jit(solution)/shard_map/all_to_all | solution.py:245
  33.7 0.0 copy-start.3
  33.7 0.0 collective-permute-start.1
  33.7 0.6 pad_add_fusion.5.meta_ref
  34.3 0.0 collective-permute-done.w_ref
  34.3 5.6 %queries.3 = bf16[384,1024]{1,0:T(8,128)(2,1)} custom-call(s32[1]{0:T(128)} %bitcast.2.core_ref, bf16[2,2,192,2048]{3,2,1,0:T(8,128)(2,1)} %bitcast.46, bf16[2048,1024]{1,0:T(8,128)(2,1)} %collective-permute-done.w_ref), custom_call_target="tpu_custom_call" | custom-call | flops 1610612736 | bytes 4194304 | tf_op jit(solution)/shard_map/queries/pallas_call | solution.py:54
  39.9 0.0 collective-permute-done.1.r2_ref
  39.9 0.0 copy-start.6
  39.9 0.0 copy-done.3
  39.9 0.7 copy-done.6
  40.6 4.6 %attend.4 = (bf16[1,64,2048]{2,1,0:T(8,128)(2,1)}, f32[1,64,8]{2,1,0:T(8,128)}) custom-call(s32[2]{0:T(128)} %get-tuple-element.21.meta_ref, bf16[2,3,64,1024]{3,2,1,0:T(8,128)(2,1)} %bitcast.49, bf16[2,3,64,1024]{3,2,1,0:T(8,128)(2,1)} %bitcast.52, bf16[768,256]{1,0:T(8,128)(2,1)} %latents.1.own_ref, bf16[512,256]{1,0:T(8,128)(2,1)} %bitcast.60, ...), custom_call_target="tpu_custom_call" | custom-call | flops 939524096 | bytes 917504 | tf_op jit(solution)/shard_map/attend/pallas_call | solution.py:173
  45.2 0.8 copy.37
  46.0 6.7 %attend.5 = (bf16[2,64,2048]{2,1,0:T(8,128)(2,1)}, f32[2,64,8]{2,1,0:T(8,128)}) custom-call(s32[2]{0:T(128)} %pad_add_fusion.5.meta_ref, bf16[2,3,64,1024]{3,2,1,0:T(8,128)(2,1)} %bitcast.50, bf16[2,3,64,1024]{3,2,1,0:T(8,128)(2,1)} %bitcast.53, bf16[768,256]{1,0:T(8,128)(2,1)} %latents.1.own_ref, bf16[512,256]{1,0:T(8,128)(2,1)} %bitcast.61, ...), custom_call_target="tpu_custom_call" | custom-call | flops 1879048192 | bytes 917504 | tf_op jit(solution)/shard_map/attend/pallas_call | solution.py:173
  52.7 0.9 copy.38
  53.6 0.0 copy-start.1
  53.6 8.8 %attend.3 = (bf16[3,64,2048]{2,1,0:T(8,128)(2,1)}, f32[3,64,8]{2,1,0:T(8,128)}) custom-call(s32[2]{0:T(128)} %get-tuple-element.20.meta_ref, bf16[2,3,64,1024]{3,2,1,0:T(8,128)(2,1)} %bitcast.51, bf16[2,3,64,1024]{3,2,1,0:T(8,128)(2,1)} %bitcast.54, bf16[768,256]{1,0:T(8,128)(2,1)} %latents.1.own_ref, bf16[512,256]{1,0:T(8,128)(2,1)} %bitcast.62, ...), custom_call_target="tpu_custom_call" | custom-call | flops 2818572288 | bytes 917504 | tf_op jit(solution)/shard_map/attend/pallas_call | solution.py:173
  62.5 0.9 %copy.39 = f32[1,192,8]{1,2,0:T(8,128)S(1)} copy(f32[1,192,8]{2,1,0:T(8,128)} %bitcast.65) | data formatting | bytes 12288 | tf_op jit(solution)/shard_map/stack;reshape | solution.py:293
  63.4 0.0 copy-start
  63.4 0.1 maximum_bitcast_fusion
  63.5 0.6 collective-permute-start.5
  64.1 0.0 collective-permute-done.2
  64.1 0.0 copy-done.1
  64.1 3.2 %fusion.7 = f32[128,2048]{1,0:T(8,128)S(1)} fusion(bf16[1024,2048]{1,0:T(8,128)(2,1)} %collective-permute-done.2, bf16[128,2048]{1,0:T(8,128)(2,1)S(1)} %bitcast.55), kind=kOutput, calls=%fused_computation.11 | convolution fusion | flops 536870912 | bytes 5505024 | tf_op jit(solution)/shard_map/dot_general | solution.py:272
  67.4 0.0 copy-done
  67.4 0.0 copy-start.2
  67.4 0.7 fusion.2
  68.1 1.6 %collective-permute-start.4 = (bf16[128,2048]{1,0:T(8,128)(2,1)S(1)}, bf16[128,2048]{1,0:T(8,128)(2,1)}, u32[]{:S(2)}, u32[]{:S(2)}) collective-permute-start(bf16[128,2048]{1,0:T(8,128)(2,1)S(1)} %fusion.2), channel_id=1, source_target_pairs={{0,2},{1,3},{2,0},{3,1},{4,6},{5,7},{6,4},{7,5},{8,10},{9,11},{10,... | collective-permute-start | bytes 1572872 | tf_op jit(solution)/shard_map/ppermute | solution.py:283
  69.7 0.0 copy-done.2
  69.7 0.0 copy-start.4
  69.7 3.1 %fusion.10 = f32[64,2048]{1,0:T(8,128)S(1)} fusion(bf16[1024,2048]{1,0:T(8,128)(2,1)} %collective-permute-done.2, bf16[64,2048]{1,0:T(8,128)(2,1)S(1)} %bitcast.57), kind=kOutput, calls=%fused_computation.14 | convolution fusion | flops 268435456 | bytes 4849664 | tf_op jit(solution)/shard_map/dot_general | solution.py:272
  72.8 0.9 fusion.3
  73.7 0.6 collective-permute-start.3
  74.3 0.0 copy-done.4
  74.3 3.2 %fusion.4 = f32[192,2048]{1,0:T(8,128)S(1)} fusion(bf16[1024,2048]{1,0:T(8,128)(2,1)} %collective-permute-done.2, bf16[192,2048]{1,0:T(8,128)(2,1)S(1)} %bitcast.63), kind=kOutput, calls=%fused_computation.8 | convolution fusion | flops 805306368 | bytes 6160384 | tf_op jit(solution)/shard_map/dot_general | solution.py:272
  77.4 0.0 collective-permute-done.5
  77.5 0.7 select_n.96
  78.2 9.5 %collective-permute-done.3 = bf16[64,2048]{1,0:T(8,128)(2,1)S(1)} collective-permute-done((bf16[64,2048]{1,0:T(8,128)(2,1)S(1)}, bf16[64,2048]{1,0:T(8,128)(2,1)S(1)}, u32[]{:S(2)}, u32[]{:S(2)}) %collective-permute-start.3) | collective-permute-done | bytes 262176 | tf_op jit(solution)/shard_map/ppermute | solution.py:283
  87.6 0.0 collective-permute-done.4
  87.7 4.2 %fusion.1 = bf16[192,2048]{1,0:T(8,128)(2,1)} fusion(f32[192,2048]{1,0:T(8,128)S(1)} %fusion.4, bf16[1024,2048]{1,0:T(8,128)(2,1)} %param.10, bf16[128,2048]{1,0:T(8,128)(2,1)} %collective-permute-done.4, bf16[64,2048]{1,0:T(8,128)(2,1)S(1)} %collective-permute-done.3, bf16[192,2048]{1,0:T(8,128)(2,1)S(1)} %bitcast.64), kind=kOutput, calls=%fused_computation.3 | convolution fusion | flops 808058880 | bytes 7733248 | tf_op jit(solution)/shard_map/dot_general | solution.py:271
  (12 shorter events, 0.1 us)
Async XLA Ops:
  0.6 14.6 %copy-start.5 = (s32[12,32]{1,0:T(8,128)S(1)}, s32[12,32]{1,0:T(8,128)}, u32[]{:S(2)}) copy-start(s32[12,32]{1,0:T(8,128)} %param.11) | copy-start | bytes 4612
  0.6 33.6 %collective-permute-start = (bf16[2048,1024]{1,0:T(8,128)(2,1)}, bf16[2048,1024]{1,0:T(8,128)(2,1)}, u32[]{:S(2)}, u32[]{:S(2)}) collective-permute-start(bf16[2048,1024]{1,0:T(8,128)(2,1)} %w_ref.2), channel_id=1, source_target_pairs={{0,1},{1,0},{2,3},{3,2},{4,5},{5,4},{6,7},{7,6},{8,9},{9,8},{10,11... | collective-permute-start | bytes 12582920 | tf_op jit(solution)/shard_map/ppermute | solution.py:226
  1.2 62.9 %collective-permute-start.2 = (bf16[1024,2048]{1,0:T(8,128)(2,1)}, bf16[1024,2048]{1,0:T(8,128)(2,1)}, u32[]{:S(2)}, u32[]{:S(2)}) collective-permute-start(bf16[1024,2048]{1,0:T(8,128)(2,1)} %param.10), channel_id=1, source_target_pairs={{0,1},{1,0},{2,3},{3,2},{4,5},{5,4},{6,7},{7,6},{8,9},{9,8},{10,11... | collective-permute-start | bytes 12582920 | tf_op jit(solution)/shard_map/ppermute | solution.py:227
  3.0 13.7 %all-to-all-start = ((s32[8,1,2]{2,1,0:T(1,128)}), s32[8,1,2]{2,1,0:T(1,128)S(1)}, u32[]{:S(2)}, u32[]{:S(2)}) async-start(s32[8,1,2]{2,1,0:T(1,128)} %copy.35), calls=%async_computation | async-start | bytes 8192 | tf_op jit(solution)/shard_map/all_to_all | solution.py:235
  19.7 13.9 %all-to-all-start.1 = ((bf16[8,2,32,256]{3,2,1,0:T(8,128)(2,1)}), bf16[8,2,32,256]{3,2,1,0:T(8,128)(2,1)S(1)}, u32[]{:S(2)}, u32[]{:S(2)}) async-start(bf16[8,2,32,256]{3,2,1,0:T(8,128)(2,1)} %bitcast.48), calls=%async_computation.1 | async-start | bytes 524288 | tf_op jit(solution)/shard_map/all_to_all | solution.py:245
  33.7 6.2 %copy-start.3 = (bf16[8,2,32,256]{3,2,1,0:T(8,128)(2,1)}, bf16[8,2,32,256]{3,2,1,0:T(8,128)(2,1)S(1)}, u32[]{:S(2)}) copy-start(bf16[8,2,32,256]{3,2,1,0:T(8,128)(2,1)S(1)} %all-to-all-done.1) | copy-start | bytes 786436
  33.7 6.2 %collective-permute-start.1 = (bf16[512,256]{1,0:T(8,128)(2,1)S(1)}, bf16[512,256]{1,0:T(8,128)(2,1)S(1)}, u32[]{:S(2)}, u32[]{:S(2)}) collective-permute-start(bf16[512,256]{1,0:T(8,128)(2,1)S(1)} %bitcast.59), channel_id=1, source_target_pairs={{0,1},{1,0},{2,3},{3,2},{4,5},{5,4},{6,7},{7,6},{8,9},{9,8},{10,11... | collective-permute-start | bytes 786440 | tf_op jit(solution)/shard_map/ppermute | solution.py:249
  39.9 0.7 copy-start.6
  53.6 10.5 %copy-start.1 = (bf16[2,64,2048]{2,1,0:T(8,128)(2,1)S(1)}, bf16[2,64,2048]{2,1,0:T(8,128)(2,1)}, u32[]{:S(2)}) copy-start(bf16[2,64,2048]{2,1,0:T(8,128)(2,1)} %get-tuple-element.10) | copy-start | bytes 1572868
  63.4 4.0 %copy-start = (bf16[1024,2048]{1,0:T(8,128)(2,1)S(1)}, bf16[1024,2048]{1,0:T(8,128)(2,1)}, u32[]{:S(2)}) copy-start(bf16[1024,2048]{1,0:T(8,128)(2,1)} %param.10) | copy-start | bytes 12582916
  63.5 13.9 %collective-permute-start.5 = (f32[2,192,4]{1,2,0:T(4,128)S(1)}, f32[2,192,4]{1,2,0:T(4,128)S(1)}, u32[]{:S(2)}, u32[]{:S(2)}) collective-permute-start(f32[2,192,4]{1,2,0:T(4,128)S(1)} %get-tuple-element.17), channel_id=1, source_target_pairs={{0,1},{1,0},{2,3},{3,2},{4,5},{5,4},{6,7},{7,6},{8,9},{9,8},{10,11... | collective-permute-start | bytes 18440 | tf_op jit(solution)/shard_map/ppermute | solution.py:295
  67.4 2.3 %copy-start.2 = (bf16[1,64,2048]{2,1,0:T(8,128)(2,1)S(1)}, bf16[1,64,2048]{2,1,0:T(8,128)(2,1)}, u32[]{:S(2)}) copy-start(bf16[1,64,2048]{2,1,0:T(8,128)(2,1)} %get-tuple-element.9) | copy-start | bytes 786436
  68.1 19.5 %collective-permute-start.4 = (bf16[128,2048]{1,0:T(8,128)(2,1)S(1)}, bf16[128,2048]{1,0:T(8,128)(2,1)}, u32[]{:S(2)}, u32[]{:S(2)}) collective-permute-start(bf16[128,2048]{1,0:T(8,128)(2,1)S(1)} %fusion.2), channel_id=1, source_target_pairs={{0,2},{1,3},{2,0},{3,1},{4,6},{5,7},{6,4},{7,5},{8,10},{9,11},{10,... | collective-permute-start | bytes 1572872 | tf_op jit(solution)/shard_map/ppermute | solution.py:283
  69.7 4.6 %copy-start.4 = (bf16[3,64,2048]{2,1,0:T(8,128)(2,1)S(1)}, bf16[3,64,2048]{2,1,0:T(8,128)(2,1)}, u32[]{:S(2)}) copy-start(bf16[3,64,2048]{2,1,0:T(8,128)(2,1)} %get-tuple-element.8) | copy-start | bytes 2359300
  73.7 14.0 %collective-permute-start.3 = (bf16[64,2048]{1,0:T(8,128)(2,1)S(1)}, bf16[64,2048]{1,0:T(8,128)(2,1)S(1)}, u32[]{:S(2)}, u32[]{:S(2)}) collective-permute-start(bf16[64,2048]{1,0:T(8,128)(2,1)S(1)} %fusion.3), channel_id=1, source_target_pairs={{0,2},{1,3},{2,0},{3,1},{4,6},{5,7},{6,4},{7,5},{8,10},{9,11},{10,... | collective-permute-start | bytes 786440 | tf_op jit(solution)/shard_map/ppermute | solution.py:283

commit v2 on v1

v2 whole, which is shorter than its diff:
```python
import functools
import math

import jax
import jax.numpy as jnp
from jax import lax
from jax.experimental import pallas as pl
from jax.experimental.pallas import tpu as pltpu
from jax.sharding import PartitionSpec as P


CAP = 2
NEG = -1e30
epsilon = 1e-06
VMEM = pltpu.VMEM
DMA = pltpu.SemaphoreType.DMA
ANY = pl.BlockSpec(memory_space=pltpu.HBM)
ON_CHIP = pl.BlockSpec(memory_space=VMEM)
SCALARS = pl.BlockSpec(memory_space=pltpu.SMEM)
VMEM_ALL = 60 * 1024 * 1024
VMEM_MOST = 64600 * 1024


def latent_kernel(tok_hbm, w_hbm, gain_hbm, out_ref, tok_v, w_v, gain_v, sems):
    parts, tile, _ = tok_v.shape
    copies = [pltpu.make_async_copy(w_hbm, w_v, sems.at[parts])]
    for i in range(parts):
        copies.append(pltpu.make_async_copy(tok_hbm.at[pl.ds(i * tile, tile)], tok_v.at[i], sems.at[i]))
    copies.append(pltpu.make_async_copy(gain_hbm, gain_v, sems.at[parts + 1]))
    for copy in copies:
        copy.start()
    copies[0].wait()
    copies[-1].wait()
    for i in range(parts):
        copies[1 + i].wait()
        projected = jnp.dot(tok_v[i], w_v[...], preferred_element_type=jnp.float32)
        inv_rms = lax.rsqrt(jnp.mean(projected * projected, axis=-1, keepdims=True) + epsilon)
        out = projected * inv_rms * gain_v[...]
        out_ref[i * tile : (i + 1) * tile, :] = out.astype(out_ref.dtype)


def latents_of(tokens, w_latent, latent_gain):
    rows, width = tokens.shape
    rank = w_latent.shape[1]
    tile = math.gcd(rows, 256)
    return pl.pallas_call(
        latent_kernel,
        in_specs=[ANY, ANY, ANY],
        out_specs=ON_CHIP,
        out_shape=jax.ShapeDtypeStruct((rows, rank), jnp.bfloat16),
        scratch_shapes=[
            VMEM((rows // tile, tile, width), jnp.bfloat16),
            VMEM((width, rank), jnp.bfloat16),
            VMEM((1, rank), jnp.float32),
            DMA((rows // tile + 2,)),
        ],
        cost_estimate=pl.CostEstimate(
            flops=2 * rows * width * rank, bytes_accessed=2 * rows * width, transcendentals=rows
        ),
        compiler_params=pltpu.CompilerParams(vmem_limit_bytes=VMEM_MOST),
        name="latents",
    )(tokens, w_latent, latent_gain.reshape(1, rank))


def query_kernel(tok_hbm, wa_hbm, wb_hbm, oa_hbm, ob_hbm, tok_v, w_v, o_v, tok_sem, w_sem, o_sem):
    m, tile, _ = tok_v.shape
    tiles = w_v.shape[0] // 2
    step = w_v.shape[2]
    core = lax.rem(lax.axis_index("tp"), 2)
    toks = [
        pltpu.make_async_copy(tok_hbm.at[i, core], tok_v.at[i], tok_sem.at[i]) for i in range(m)
    ]
    loads = [
        pltpu.make_async_copy(
            w_hbm.at[:, pl.ds(n * step, step)], w_v.at[u * tiles + n], w_sem.at[u * tiles + n]
        )
        for u, w_hbm in enumerate((wa_hbm, wb_hbm))
        for n in range(tiles)
    ]
    stores = [
        pltpu.make_async_copy(
            o_v.at[u * tiles + n], o_hbm.at[:, pl.ds(n * step, step)], o_sem.at[u * tiles + n]
        )
        for u, o_hbm in enumerate((oa_hbm, ob_hbm))
        for n in range(tiles)
    ]
    for copy in toks + loads[:2]:
        copy.start()
    for n in range(2 * tiles):
        if n + 2 < 2 * tiles:
            loads[n + 2].start()
        loads[n].wait()
        for i in range(m):
            if n == 0:
                toks[i].wait()
            out = jnp.dot(tok_v[i], w_v[n], preferred_element_type=jnp.float32)
            o_v[n, i * tile : (i + 1) * tile, :] = out.astype(o_v.dtype)
        stores[n].start()
    for copy in stores:
        copy.wait()


def queries_of(tokens4, wq_a, wq_b):
    m, _, tile, width = tokens4.shape
    cols = wq_a.shape[1]
    step = math.gcd(cols, 512)
    tiles = cols // step
    shape = jax.ShapeDtypeStruct((m * tile, cols), jnp.bfloat16)
    return pl.pallas_call(
        query_kernel,
        in_specs=[ANY, ANY, ANY],
        out_specs=[ANY, ANY],
        scratch_shapes=[
            VMEM((m, tile, width), jnp.bfloat16),
            VMEM((2 * tiles, width, step), jnp.bfloat16),
            VMEM((2 * tiles, m * tile, step), jnp.bfloat16),
            DMA((m,)),
            DMA((2 * tiles,)),
            DMA((2 * tiles,)),
        ],
        out_shape=[shape, shape],
        cost_estimate=pl.CostEstimate(
            flops=4 * m * tile * width * cols,
            bytes_accessed=4 * width * cols,
            transcendentals=0,
        ),
        compiler_params=pltpu.CompilerParams(vmem_limit_bytes=VMEM_ALL),
        name="queries",
    )(tokens4, wq_a, wq_b)


def pick_kernel(asked_ref, lat_ref, out_ref):
    per_device = lat_ref.shape[0]
    owners, _, count = asked_ref.shape
    first = lax.axis_index("kv") * per_device
    core = lax.rem(lax.axis_index("tp"), 2)
    for i in range(owners):
        for j in range(count):
            block = jnp.clip(asked_ref[i, 0, j] - first, 0, per_device - 1)
            out_ref[i, j] = lat_ref[block, core]


def pick_halves(asked, latent4):
    _, _, half, rank = latent4.shape
    owners, _, count = asked.shape
    return pl.pallas_call(
        pick_kernel,
        in_specs=[SCALARS, ON_CHIP],
        out_specs=ON_CHIP,
        out_shape=jax.ShapeDtypeStruct((owners, count, half, rank), latent4.dtype),
        compiler_params=pltpu.CompilerParams(vmem_limit_bytes=VMEM_MOST),
        name="pick",
    )(asked, latent4)


def project_kernel(ho_hbm, wa_hbm, wb_hbm, out_hbm, ho_v, w_v, out_v, sems, w_sem, out_sem):
    tiles, _, _, step = w_v.shape
    begin = wa_hbm.shape[1] - tiles * step
    hos = [pltpu.make_async_copy(ho_hbm.at[u], ho_v.at[u], sems.at[u]) for u in range(2)]
    for copy in hos:
        copy.start()
    finish_project(begin, ho_v, wa_hbm, wb_hbm, out_hbm, w_v, out_v, w_sem, out_sem, hos)


def finish_project(begin, ho_v, wa_hbm, wb_hbm, out_hbm, w_v, out_v, w_sem, out_sem, hos):
    weights = project_loads(begin, wa_hbm, wb_hbm, w_v, w_sem)
    for copy in weights:
        copy.start()
    for copy in hos:
        copy.wait()
    project_tiles(weights, ho_v, out_hbm, w_v, out_v, out_sem)


def project_loads(begin, wa_hbm, wb_hbm, w_v, w_sem):
    tiles, _, _, step = w_v.shape
    return [
        pltpu.make_async_copy(w_hbm.at[:, pl.ds(begin + n * step, step)], w_v.at[n, u], w_sem.at[n, u])
        for n in range(tiles)
        for u, w_hbm in enumerate((wa_hbm, wb_hbm))
    ]


def project_tiles(weights, ho_v, out_hbm, w_v, out_v, out_sem):
    tiles, _, step = out_v.shape
    stores = []
    for n in range(tiles):
        weights[2 * n].wait()
        weights[2 * n + 1].wait()
        total = jnp.dot(ho_v[0], w_v[n, 0], preferred_element_type=jnp.float32)
        total = total + jnp.dot(ho_v[1], w_v[n, 1], preferred_element_type=jnp.float32)
        out_v[n] = total.astype(out_v.dtype)
        store = pltpu.make_async_copy(out_v.at[n], out_hbm.at[:, pl.ds(n * step, step)], out_sem.at[n])
        store.start()
        stores.append(store)
    for store in stores:
        store.wait()


def project(ho, wo_a, wo_b, width):
    _, rows, cols = ho.shape
    step = math.gcd(width, 512)
    tiles = width // step
    return pl.pallas_call(
        project_kernel,
        in_specs=[ANY] * 3,
        out_specs=ANY,
        scratch_shapes=[
            VMEM((2, rows, cols), jnp.bfloat16),
            VMEM((tiles, 2, cols, step), jnp.bfloat16),
            VMEM((tiles, rows, step), jnp.bfloat16),
            DMA((2,)),
            DMA((tiles, 2)),
            DMA((tiles,)),
        ],
        out_shape=jax.ShapeDtypeStruct((rows, width), jnp.bfloat16),
        cost_estimate=pl.CostEstimate(
            flops=4 * rows * cols * width, bytes_accessed=4 * cols * width, transcendentals=0
        ),
        compiler_params=pltpu.CompilerParams(vmem_limit_bytes=VMEM_ALL),
        name="project",
    )(ho, wo_a, wo_b)


def finish_kernel(own_ref, *refs):
    pieces, (out_hbm, out_v, sems) = refs[:-3], refs[-3:]
    halves, _, part = out_v.shape
    stores = []
    for h in range(halves):
        total = own_ref[:, h * part : (h + 1) * part].astype(jnp.float32)
        for piece in pieces[h::halves]:
            total = total + piece[...].astype(jnp.float32)
        out_v[h] = total.astype(out_v.dtype)
        stores.append(
            pltpu.make_async_copy(out_v.at[h], out_hbm.at[:, pl.ds(h * part, part)], sems.at[h])
        )
        stores[h].start()
    for copy in stores:
        copy.wait()


def finish(own, pieces):
    rows, width = own.shape
    part = width // 2
    return pl.pallas_call(
        finish_kernel,
        in_specs=[ON_CHIP] * (1 + len(pieces)),
        out_specs=ANY,
        out_shape=jax.ShapeDtypeStruct((rows, width), own.dtype),
        scratch_shapes=[VMEM((2, rows, part), own.dtype), DMA((2,))],
        compiler_params=pltpu.CompilerParams(vmem_limit_bytes=12 << 20),
        name="finish",
    )(own, *pieces)


def attend_kernel(
    scale,
    ahead,
    named_hbm,
    qa_hbm,
    qb_hbm,
    own_hbm,
    r1_hbm,
    r2_hbm,
    wa_hbm,
    wb_hbm,
    out_hbm,
    ho_hbm,
    lse_hbm,
    named_ref,
    q_v,
    key_v,
    val_v,
    w_v,
    out_v,
    s0_ref,
    s1_ref,
    p0_ref,
    p1_ref,
    bl_ref,
    ho_ref,
    lse_ref,
    sems,
    w_sem,
    out_sem,
    ho_sem,
):
    _, count, blk_len, cols = q_v.shape
    key_len, rank = key_v.shape
    heads = cols // rank
    own_len = own_hbm.shape[0]
    rem_len = r1_hbm.shape[0]
    half = blk_len // 2
    own_blocks = own_len // blk_len
    slots = rem_len // half
    lanes = bl_ref.shape[2]
    unit = heads * blk_len
    exp_scale = scale * math.log2(math.e)
    tp = lax.axis_index("tp")
    chip = lax.rem(tp // 2 + ahead, qa_hbm.shape[0])
    first = (chip * 2 + lax.rem(tp, 2)) * count
    naming = pltpu.make_async_copy(named_hbm, named_ref, sems.at[5])
    parts = []
    base = 0
    for i, hbm in enumerate((own_hbm, r1_hbm, r2_hbm)):
        n = hbm.shape[0]
        parts.append((pltpu.make_async_copy(hbm, key_v.at[pl.ds(base, n)], sems.at[2 + i]), base, n))
        base += n
    qs = [
        pltpu.make_async_copy(q_hbm.at[chip], q_v.at[u], sems.at[u])
        for u, q_hbm in enumerate((qa_hbm, qb_hbm))
    ]
    weights = project_loads(0, wa_hbm, wb_hbm, w_v, w_sem)
    for copy in [naming, qs[0], parts[0][0], parts[1][0], parts[2][0], qs[1]]:
        copy.start()

    naming.wait()

    def own_bias(b, _):
        k_off = lax.broadcasted_iota(jnp.int32, (blk_len, lanes), 0)
        q_off = lax.broadcasted_iota(jnp.int32, (blk_len, lanes), 1) % blk_len
        here = first + b
        for j in range(own_blocks):
            keep = k_off + (j - here) * blk_len <= q_off
            bl_ref[b, j * blk_len : (j + 1) * blk_len, :] = jnp.where(keep, named_ref[here, j], NEG)
        return 0

    lax.fori_loop(0, count, own_bias, 0)
    chunk = math.gcd(math.gcd(own_len, rem_len), 256)
    for copy in [part[0] for part in parts] + qs:
        copy.wait()
    for copy in weights:
        copy.start()
    for k in range(0, key_len, chunk):
        val_v[:, k : k + chunk] = key_v[k : k + chunk, :].T

    def scores(b, u, s_ref):
        here = first + b
        q = jnp.concatenate(
            [q_v[u, b, :, h * rank : (h + 1) * rank] for h in range(heads)], axis=0
        )
        peak = jnp.full((8, unit), NEG, jnp.float32)
        for at in range(0, key_len, chunk):
            s = lax.dot_general(
                key_v[at : at + chunk, :], q, (((1,), (1,)), ((), ())), preferred_element_type=jnp.float32
            )
            for k in range(0, chunk, half):
                col = at + k
                row = s[k : k + half]
                if col < own_len:
                    add = bl_ref[b, col : col + half, :]
                    row = row + jnp.concatenate([add] * (unit // lanes), axis=1)
                else:
                    row = row + named_ref[here, own_blocks + (col - own_len) // half % slots]
                s_ref[col : col + half, :] = row
                for r in range(0, half, 8):
                    peak = jnp.maximum(peak, row[r : r + 8])
        return jnp.max(peak, axis=0, keepdims=True)

    def weigh(b, u, s_ref, p_ref, peak):
        mass = jnp.zeros((8, unit), jnp.float32)
        for k in range(0, key_len, half):
            raised = jnp.exp2((s_ref[k : k + half, :] - peak) * exp_scale)
            p_ref[k : k + half, :] = raised.astype(p_ref.dtype)
            for r in range(0, half, 8):
                mass = mass + raised[r : r + 8]
        mass = jnp.sum(mass, axis=0, keepdims=True)
        lse_ref[b, u : u + 1, :] = peak * scale + jnp.log(mass)
        return 1.0 / mass

    def gather(b, u, p_ref, inverse):
        out = jnp.dot(val_v[...], p_ref[...], preferred_element_type=jnp.float32)
        out = (out * inverse).astype(ho_ref.dtype).T
        at = pl.multiple_of(b * blk_len, blk_len)
        for h in range(heads):
            ho_ref[u, pl.ds(at, blk_len), h * rank : (h + 1) * rank] = out[h * blk_len : (h + 1) * blk_len]

    def block(b, carry):
        peak0, inverse1 = carry
        peak1 = scores(b, 1, s1_ref)
        inverse0 = weigh(b, 0, s0_ref, p0_ref, peak0)
        gather(jnp.maximum(b - 1, 0), 1, p1_ref, inverse1)
        after = scores(jnp.minimum(b + 1, count - 1), 0, s0_ref)
        inverse1 = weigh(b, 1, s1_ref, p1_ref, peak1)
        gather(b, 0, p0_ref, inverse0)
        return after, inverse1

    p1_ref[...] = jnp.zeros_like(p1_ref)
    start = (scores(0, 0, s0_ref), jnp.ones((1, unit), jnp.float32))
    _, inverse1 = lax.fori_loop(0, count, block, start)
    gather(count - 1, 1, p1_ref, inverse1)
    keeps = [
        pltpu.make_async_copy(ho_ref, ho_hbm, ho_sem.at[0]),
        pltpu.make_async_copy(lse_ref, lse_hbm, ho_sem.at[1]),
    ]
    for copy in keeps:
        copy.start()
    project_tiles(weights, ho_ref, out_hbm, w_v, out_v, out_sem)
    for copy in keeps:
        copy.wait()


def attend(named, qa, qb, latent, r1, r2, wo_a, wo_b, width, ahead, scale):
    _, count, blk_len, cols = qa.shape
    own_len, rank = latent.shape
    heads = cols // rank
    key_len = own_len + 2 * r1.shape[0]
    step = math.gcd(width, 512)
    tiles = width // step
    unit = heads * blk_len
    return pl.pallas_call(
        functools.partial(attend_kernel, scale, ahead),
        in_specs=[ANY] * 8,
        out_specs=[ANY] * 3,
        scratch_shapes=[
                pltpu.SMEM(named.shape, jnp.float32),
                VMEM((2, count, blk_len, cols), jnp.bfloat16),
                VMEM((key_len, rank), jnp.bfloat16),
                VMEM((rank, key_len), jnp.bfloat16),
                VMEM((tiles, 2, cols, step), jnp.bfloat16),
                VMEM((tiles, count * blk_len, step), jnp.bfloat16),
                VMEM((key_len, unit), jnp.float32),
                VMEM((key_len, unit), jnp.float32),
                VMEM((key_len, unit), jnp.bfloat16),
                VMEM((key_len, unit), jnp.bfloat16),
                VMEM((count, own_len, 2 * blk_len), jnp.float32),
                VMEM((2, count * blk_len, cols), jnp.bfloat16),
                VMEM((count, 2, unit), jnp.float32),
                DMA((6,)),
                DMA((tiles, 2)),
                DMA((tiles,)),
                DMA((2,)),
        ],
        out_shape=[
            jax.ShapeDtypeStruct((count * blk_len, width), jnp.bfloat16),
            jax.ShapeDtypeStruct((2, count * blk_len, cols), jnp.bfloat16),
            jax.ShapeDtypeStruct((count, 2, unit), jnp.float32),
        ],
        cost_estimate=pl.CostEstimate(
            flops=8 * count * unit * key_len * rank + 4 * count * blk_len * cols * width,
            bytes_accessed=2 * key_len * rank + 4 * cols * width,
            transcendentals=2 * count * unit * key_len,
        ),
        compiler_params=pltpu.CompilerParams(vmem_limit_bytes=VMEM_ALL),
        name="attend",
    )(named, qa, qb, latent, r1, r2, wo_a, wo_b)


def layer(tokens, w_query, w_latent, latent_gain, w_output, chosen):
    tok_rows, width = tokens.shape
    rank = w_latent.shape[1]
    heads = w_query.shape[1] // rank
    per_device, picks = chosen.shape
    blk_len = tok_rows // per_device
    half = blk_len // 2
    devices = lax.axis_size("kv")
    n_tp = lax.axis_size("tp")
    m = n_tp // 2
    tile_rows = tok_rows // n_tp
    tile_blocks = tile_rows // blk_len
    mine = lax.axis_index("kv")
    tp = lax.axis_index("tp")
    chip, core = tp // 2, tp % 2
    swap = [(i, i ^ 1) for i in range(n_tp)]

    wq_other = lax.ppermute(w_query, "tp", swap)

    flat = chosen.reshape(1, per_device * picks)
    first_id = (jnp.arange(devices, dtype=jnp.int32) * per_device)[:, None]
    of_owner = (flat >= first_id) & (flat < first_id + per_device)
    low = jnp.min(jnp.where(of_owner, flat, devices * per_device), axis=1)
    high = jnp.max(jnp.where(of_owner, flat, -1), axis=1)
    request = jnp.stack([low, high], axis=1)[:, None, :]
    asked = lax.all_to_all(request, "kv", split_axis=0, concat_axis=0, tiled=True)

    latent = latents_of(tokens, w_latent, latent_gain)
    held, latent = lax.optimization_barrier((w_output, latent))
    wo_other = lax.ppermute(held, "tp", swap)
    tokens4 = tokens.reshape(m, 2, tile_rows, width)

    reply = pick_halves(asked, latent.reshape(per_device, 2, half, rank))
    fetched = lax.all_to_all(
        reply, "kv", split_axis=0, concat_axis=0, tiled=True
    )
    r1 = fetched.reshape(devices * CAP * half, rank)
    r2 = lax.ppermute(r1, "tp", swap)
    qa, qb = queries_of(tokens4, w_query, wq_other)

    earlier = jnp.arange(devices, dtype=jnp.int32) < mine
    slots = jnp.stack(
        [jnp.where(earlier, low, -2), jnp.where(earlier & (high > low), high, -2)], axis=1
    ).reshape(devices * CAP)
    own_ids = mine * per_device + jnp.arange(per_device, dtype=jnp.int32)
    key_ids = jnp.concatenate([own_ids, slots])
    named = jnp.any(chosen[:, :, None] == key_ids[None, None, :], axis=1)
    named = jnp.where(named, 0.0, NEG).astype(jnp.float32)

    qa4 = qa.reshape(m, tile_blocks, blk_len, heads * rank)
    qb4 = qb.reshape(m, tile_blocks, blk_len, heads * rank)
    scale = rank ** (-0.5)

    def work(k, cols):
        out, ho, lse = attend(named, qa4, qb4, latent, r1, r2, w_output, wo_other, cols, k, scale)
        return out, ho, lse.reshape(tile_blocks, 2, heads, blk_len)

    lse_tiles = [None] * m
    arrived = []
    part = width // 2
    for k in range(1, m):
        to_chip = [(i, (i + 2 * k) % n_tp) for i in range(n_tp)]
        out0, ho, lse_tiles[k] = work(k, part)
        piece0 = lax.ppermute(out0, "tp", to_chip)
        out1 = project(ho, w_output, wo_other, width - part)
        piece1 = lax.ppermute(out1, "tp", to_chip)
        arrived.append([piece0, piece1])
    total, _, lse_tiles[0] = work(0, width)
    attended = finish(total, sum(arrived, []))

    lse = jnp.stack(lse_tiles)
    lse = lax.dynamic_slice_in_dim(jnp.concatenate([lse, lse], axis=0), (m - chip) % m, m, 0)
    theirs = lax.ppermute(lse[:, :, 1], "tp", swap)
    ours = lse[:, :, 0]
    log_total = jnp.where(
        core == 0, jnp.stack([ours, theirs], axis=1), jnp.stack([theirs, ours], axis=1)
    )
    log_total = jnp.swapaxes(log_total, 3, 4).reshape(tok_rows, heads)
    return (attended, log_total)


def solution(mesh):
    placed = (P("kv", None), P(None, "tp"), P(), P(), P("tp", None), P("kv", None))
    return jax.shard_map(
        layer,
        mesh=mesh,
        in_specs=placed,
        out_specs=(P(("kv", "tp"), None), P("kv", "tp")),
        check_vma=False,
    )
```

time: 92.7 us -> 76.7 us (0.83)
  matrix products: 15.3 us -> 0 us
  waiting for transfers between devices: 11.7 us -> 14.7 us
  Pallas kernels: 38.3 us -> 40.9 us
  starting transfers between devices: 16 us -> 13.6 us
  local copies, waits for them, and re-layouts: 6.77 us -> 4.91 us
  other arithmetic: 2.92 us -> 1.14 us
    dot_general x6 -> x0, matrix products: 15.3 us -> none  [the longest x3 9.51 us: work(): jnp.dot(ho[:, heads * rank:], wo_other, preferred_element_type=jnp.float32)]
    all_to_all x2, waiting for transfers between devices: 2.27 us -> 13.5 us  [the longest x1 7.12 us: layer(): lax.all_to_all(reply, 'kv', split_axis=0, concat_axis=0, tiled=True)]
    ppermute x6, waiting for transfers between devices: 9.48 us -> 1.17 us  [the longest x1 1.16 us: layer(): theirs = lax.ppermute(lse[:, :, 1], 'tp', swap)]
    pallas_call x7, Pallas kernels: 38.3 us -> 40.9 us  [the longest x2 21.2 us: attend(): pl.pallas_call(functools.partial(attend_kernel, scale, ahead), in_specs=[...]
    all_to_all x2, starting transfers between devices: 12.6 us -> 10.7 us  [the longest x1 7.3 us: layer(): lax.all_to_all(request, 'kv', split_axis=0, concat_axis=0, tiled=True)]
    unnamed x14 -> x12, local copies, waits for them, and re-layouts: 0.74 us -> 2.42 us
    select_n x3 -> x0, local copies, waits for them, and re-layouts: 1.39 us -> none  [the longest x2 0.7 us: local(): jnp.where(core == 0, jnp.stack([ours, theirs], axis=1), jnp.stack([theirs...]
    another operation x4 -> x1, other arithmetic: 1.33 us -> 0.01 us  [layer(): jnp.stack([jnp.where(earlier, low, -2), jnp.where(earlier & (high > low),...]
  transfers between devices with their start and end apart: 8 -> 8, of which waited for: 3 -> 3; matrix products, arithmetic and copies ran while one was open for 22% -> 5% of each run, Pallas kernels for 42% -> 40%
where the time goes in v2:
time: 76.7 us; the launch traced here: 76.3 us
  Pallas kernels  40.9 us (53%)
  waiting for transfers between devices  14.7 us (19%)
  starting transfers between devices  13.6 us (18%)
  local copies, waits for them, and re-layouts  4.91 us (6%)
  other arithmetic  1.14 us (1%)
  between operations  1.01 us (1%)
    pallas_call x2, Pallas kernels, attend(): pl.pallas_call(functools.partial(attend_kernel, scale, ahead), in_specs=[...  21.2 us
    pallas_call x1, Pallas kernels, queries_of(): pl.pallas_call(query_kernel, in_specs=[ANY, ANY, ANY], out_specs=[ANY, AN...  8.1 us
    all_to_all x1, starting transfers between devices, layer(): lax.all_to_all(request, 'kv', split_axis=0, concat_axis=0, tiled=True)  7.3 us
    all_to_all x1, waiting for transfers between devices, layer(): lax.all_to_all(reply, 'kv', split_axis=0, concat_axis=0, tiled=True)  7.12 us
    all_to_all x1, waiting for transfers between devices, layer(): lax.all_to_all(request, 'kv', split_axis=0, concat_axis=0, tiled=True)  6.39 us
    pallas_call x1, Pallas kernels, latents_of(): pl.pallas_call(latent_kernel, in_specs=[ANY, ANY, ANY], out_specs=ON_CHIP...  4.81 us
    pallas_call x1, Pallas kernels, project(): pl.pallas_call(project_kernel, in_specs=[ANY] * 3, out_specs=ANY, scratch...  4.03 us
    all_to_all x1, starting transfers between devices, layer(): lax.all_to_all(reply, 'kv', split_axis=0, concat_axis=0, tiled=True)  3.41 us
  transfers between devices with their start and end apart: 8, of which 3 were waited for; matrix products, arithmetic and copies ran while one was open for 5% of the time, Pallas kernels for 40%

profile of v2, /device:TPU:0, one launch (start us, length us, event | category | flops | bytes accessed | tf_op | source)
XLA Modules:
  0.0 76.3 jit_solution(9592001030212849697)
XLA Ops:
  0.6 0.0 copy-start.2
  0.6 0.6 collective-permute-start
  1.2 4.8 %latents.1.own_hbm = bf16[768,256]{1,0:T(8,128)(2,1)} custom-call(bf16[768,2048]{1,0:T(8,128)(2,1)} %tok_hbm.1, bf16[2048,256]{1,0:T(8,128)(2,1)} %w_hbm.1, f32[1,256]{1,0:T(1,128)} %bitcast.30), custom_call_target="tpu_custom_call" | custom-call | flops 805306368 | bytes 3145728 | tf_op jit(solution)/shard_map/latents/pallas_call | solution.py:46
  6.0 0.1 collective-permute-start.2
  6.1 0.0 copy-done.2
  6.1 0.1 ge.15
  6.2 0.2 select_reduce_fusion.1
  6.4 0.7 copy.19
  7.1 7.3 %all-to-all-start = ((s32[8,1,2]{2,1,0:T(1,128)}), s32[8,1,2]{2,1,0:T(1,128)S(1)}, u32[]{:S(2)}, u32[]{:S(2)}) async-start(s32[8,1,2]{2,1,0:T(1,128)} %copy.19), calls=%async_computation | async-start | bytes 8192 | tf_op jit(solution)/shard_map/all_to_all | solution.py:473
  14.4 6.4 %all-to-all-done.asked_ref = s32[8,1,2]{2,1,0:T(1,128)S(1)} async-done(((s32[8,1,2]{2,1,0:T(1,128)}), s32[8,1,2]{2,1,0:T(1,128)S(1)}, u32[]{:S(2)}, u32[]{:S(2)}) %all-to-all-start) | async-done | bytes 96 | tf_op jit(solution)/shard_map/all_to_all | solution.py:473
  20.8 0.0 copy-start.3
  20.8 0.6 copy-done.3
  21.4 1.8 %pick.1 = bf16[8,2,32,256]{3,2,1,0:T(8,128)(2,1)} custom-call(s32[8,1,2]{2,1,0:T(1,128)} %copy-done.3, bf16[12,2,32,256]{3,2,1,0:T(8,128)(2,1)} %bitcast.23), custom_call_target="tpu_custom_call" | custom-call | tf_op jit(solution)/shard_map/pick/pallas_call | solution.py:146
  23.2 3.4 %all-to-all-start.1 = ((bf16[8,2,32,256]{3,2,1,0:T(8,128)(2,1)}), bf16[8,2,32,256]{3,2,1,0:T(8,128)(2,1)S(1)}, u32[]{:S(2)}, u32[]{:S(2)}) async-start(bf16[8,2,32,256]{3,2,1,0:T(8,128)(2,1)} %pick.1), calls=%async_computation.1 | async-start | bytes 524288 | tf_op jit(solution)/shard_map/all_to_all | solution.py:481
  26.6 0.1 copy.18
  26.7 0.1 reshape.72
  26.8 0.1 pad_add_fusion.1
  26.9 0.1 compare_reduce_fusion
  27.0 0.6 broadcast_select_fusion.named_hbm
  27.6 7.1 %all-to-all-done.1 = bf16[8,2,32,256]{3,2,1,0:T(8,128)(2,1)S(1)} async-done(((bf16[8,2,32,256]{3,2,1,0:T(8,128)(2,1)}), bf16[8,2,32,256]{3,2,1,0:T(8,128)(2,1)S(1)}, u32[]{:S(2)}, u32[]{:S(2)}) %all-to-all-start.1) | async-done | bytes 262176 | tf_op jit(solution)/shard_map/all_to_all | solution.py:481
  34.8 0.0 copy-start.1
  34.8 0.0 collective-permute-start.1
  34.8 0.0 collective-permute-done.wb_hbm
  34.8 8.1 %queries.1 = (bf16[384,1024]{1,0:T(8,128)(2,1)}, bf16[384,1024]{1,0:T(8,128)(2,1)}) custom-call(bf16[2,2,192,2048]{3,2,1,0:T(8,128)(2,1)} %bitcast.22, bf16[2048,1024]{1,0:T(8,128)(2,1)} %wa_hbm.4, bf16[2048,1024]{1,0:T(8,128)(2,1)} %collective-permute-done.wb_hbm), custom_call_target="tpu_custom_call" | custom-call | flops 3221225472 | bytes 8388608 | tf_op jit(solution)/shard_map/queries/pallas_call | solution.py:109
  42.9 0.0 copy-done.1
  42.9 0.0 collective-permute-done.1.r2_hbm
  42.9 0.0 copy-start.5
  42.9 0.0 collective-permute-done.2.wb_hbm
  42.9 0.7 copy-done.5
  43.6 9.5 %attend.3 = (bf16[192,1024]{1,0:T(8,128)(2,1)}, bf16[2,192,1024]{2,1,0:T(8,128)(2,1)}, f32[3,2,256]{2,1,0:T(2,128)}) custom-call(f32[12,28]{1,0:T(8,128)} %broadcast_select_fusion.named_hbm, bf16[2,3,64,1024]{3,2,1,0:T(8,128)(2,1)} %bitcast.31, bf16[2,3,64,1024]{3,2,1,0:T(8,128)(2,1)} %bitcast.33, bf16[768,256]{1,0:T(8,128)(2,1)} %latents.1.own_hbm, ...), custom_call_target="tpu_custom_call" | custom-call | flops 3623878656 | bytes 5111808 | tf_op jit(solution)/shard_map/attend/pallas_call | solution.py:410
  53.1 1.6 %collective-permute-start.3 = (bf16[192,1024]{1,0:T(8,128)(2,1)}, bf16[192,1024]{1,0:T(8,128)(2,1)S(1)}, u32[]{:S(2)}, u32[]{:S(2)}) collective-permute-start(bf16[192,1024]{1,0:T(8,128)(2,1)} %get-tuple-element.16), channel_id=1, source_target_pairs={{0,2},{1,3},{2,0},{3,1},{4,6},{5,7},{6,4},{7,5},{8,10},{9,11},{10,... | collective-permute-start | bytes 1179656 | tf_op jit(solution)/shard_map/ppermute | solution.py:511
  54.7 4.0 %project.1 = bf16[192,1024]{1,0:T(8,128)(2,1)} custom-call(bf16[2,192,1024]{2,1,0:T(8,128)(2,1)} %get-tuple-element.17.ho_hbm, bf16[1024,2048]{1,0:T(8,128)(2,1)} %wa_hbm.7, bf16[1024,2048]{1,0:T(8,128)(2,1)} %collective-permute-done.2.wb_hbm), custom_call_target="tpu_custom_call" | custom-call | flops 805306368 | bytes 4194304 | tf_op jit(solution)/shard_map/project/pallas_call | solution.py:203
  58.7 0.0 copy-start.4
  58.8 0.6 collective-permute-start.4
  59.4 11.7 %attend.2 = (bf16[192,2048]{1,0:T(8,128)(2,1)}, bf16[2,192,1024]{2,1,0:T(8,128)(2,1)}, f32[3,2,256]{2,1,0:T(2,128)}) custom-call(f32[12,28]{1,0:T(8,128)} %broadcast_select_fusion.named_hbm, bf16[2,3,64,1024]{3,2,1,0:T(8,128)(2,1)} %bitcast.32, bf16[2,3,64,1024]{3,2,1,0:T(8,128)(2,1)} %bitcast.34, bf16[768,256]{1,0:T(8,128)(2,1)} %latents.1.own_hbm, ...), custom_call_target="tpu_custom_call" | custom-call | flops 4429185024 | bytes 9306112 | tf_op jit(solution)/shard_map/attend/pallas_call | solution.py:410
  71.1 0.8 %stack_reshape.6 = f32[1,3,2,4,64]{4,3,2,1,0:T(4,128)S(1)} reshape(f32[3,2,256]{2,1,0:T(2,128)} %get-tuple-element.18) | data formatting | bytes 12288 | tf_op jit(solution)/shard_map/stack;reshape | solution.py:518
  71.9 0.0 copy-done.4
  71.9 0.1 stack_reshape.7
  72.0 0.1 collective-permute-start.5
  72.1 1.2 %collective-permute-done.5 = f32[2,3,4,64]{3,1,0,2:T(4,128)S(1)} collective-permute-done((f32[2,3,4,64]{3,1,0,2:T(4,128)S(1)}, f32[2,3,4,64]{3,1,0,2:T(4,128)S(1)}, u32[]{:S(2)}, u32[]{:S(2)}) %collective-permute-start.5) | collective-permute-done | bytes 6176 | tf_op jit(solution)/shard_map/ppermute | solution.py:520
  73.3 0.7 reshape.79
  74.0 0.0 collective-permute-done.3.refs_0_
  74.0 0.0 collective-permute-done.4.refs_1_
  74.0 0.0 copy-start
  74.0 1.1 %copy-done = bf16[192,2048]{1,0:T(8,128)(2,1)S(1)} copy-done((bf16[192,2048]{1,0:T(8,128)(2,1)S(1)}, bf16[192,2048]{1,0:T(8,128)(2,1)}, u32[]{:S(2)}) %copy-start) | copy-done | bytes 786456
  75.1 1.0 %finish.1 = bf16[192,2048]{1,0:T(8,128)(2,1)} custom-call(bf16[192,2048]{1,0:T(8,128)(2,1)S(1)} %copy-done, bf16[192,1024]{1,0:T(8,128)(2,1)S(1)} %collective-permute-done.3.refs_0_, bf16[192,1024]{1,0:T(8,128)(2,1)S(1)} %collective-permute-done.4.refs_1_), custom_call_target="tpu_custom_call" | custom-call | tf_op jit(solution)/shard_map/finish/pallas_call | solution.py:244
  (10 shorter events, 0.1 us)
Async XLA Ops:
  0.6 5.5 %copy-start.2 = (s32[12,32]{1,0:T(8,128)S(1)}, s32[12,32]{1,0:T(8,128)}, u32[]{:S(2)}) copy-start(s32[12,32]{1,0:T(8,128)} %param.11) | copy-start | bytes 4612
  0.6 34.1 %collective-permute-start = (bf16[2048,1024]{1,0:T(8,128)(2,1)}, bf16[2048,1024]{1,0:T(8,128)(2,1)}, u32[]{:S(2)}, u32[]{:S(2)}) collective-permute-start(bf16[2048,1024]{1,0:T(8,128)(2,1)} %wa_hbm.4), channel_id=1, source_target_pairs={{0,1},{1,0},{2,3},{3,2},{4,5},{5,4},{6,7},{7,6},{8,9},{9,8},{10,11... | collective-permute-start | bytes 12582920 | tf_op jit(solution)/shard_map/ppermute | solution.py:465
  6.0 36.9 %collective-permute-start.2 = (bf16[1024,2048]{1,0:T(8,128)(2,1)}, bf16[1024,2048]{1,0:T(8,128)(2,1)}, u32[]{:S(2)}, u32[]{:S(2)}) collective-permute-start(bf16[1024,2048]{1,0:T(8,128)(2,1)} %wa_hbm.7), channel_id=1, source_target_pairs={{0,1},{1,0},{2,3},{3,2},{4,5},{5,4},{6,7},{7,6},{8,9},{9,8},{10,11... | collective-permute-start | bytes 12582920 | tf_op jit(solution)/shard_map/ppermute | solution.py:477
  7.1 13.7 %all-to-all-start = ((s32[8,1,2]{2,1,0:T(1,128)}), s32[8,1,2]{2,1,0:T(1,128)S(1)}, u32[]{:S(2)}, u32[]{:S(2)}) async-start(s32[8,1,2]{2,1,0:T(1,128)} %copy.19), calls=%async_computation | async-start | bytes 8192 | tf_op jit(solution)/shard_map/all_to_all | solution.py:473
  20.8 0.6 copy-start.3
  23.2 11.6 %all-to-all-start.1 = ((bf16[8,2,32,256]{3,2,1,0:T(8,128)(2,1)}), bf16[8,2,32,256]{3,2,1,0:T(8,128)(2,1)S(1)}, u32[]{:S(2)}, u32[]{:S(2)}) async-start(bf16[8,2,32,256]{3,2,1,0:T(8,128)(2,1)} %pick.1), calls=%async_computation.1 | async-start | bytes 524288 | tf_op jit(solution)/shard_map/all_to_all | solution.py:481
  34.8 8.1 %copy-start.1 = (bf16[8,2,32,256]{3,2,1,0:T(8,128)(2,1)}, bf16[8,2,32,256]{3,2,1,0:T(8,128)(2,1)S(1)}, u32[]{:S(2)}) copy-start(bf16[8,2,32,256]{3,2,1,0:T(8,128)(2,1)S(1)} %all-to-all-done.1) | copy-start | bytes 786436
  34.8 8.1 %collective-permute-start.1 = (bf16[512,256]{1,0:T(8,128)(2,1)S(1)}, bf16[512,256]{1,0:T(8,128)(2,1)S(1)}, u32[]{:S(2)}, u32[]{:S(2)}) collective-permute-start(bf16[512,256]{1,0:T(8,128)(2,1)S(1)} %bitcast.24), channel_id=1, source_target_pairs={{0,1},{1,0},{2,3},{3,2},{4,5},{5,4},{6,7},{7,6},{8,9},{9,8},{10,11... | collective-permute-start | bytes 786440 | tf_op jit(solution)/shard_map/ppermute | solution.py:485
  42.9 0.7 copy-start.5
  53.1 20.8 %collective-permute-start.3 = (bf16[192,1024]{1,0:T(8,128)(2,1)}, bf16[192,1024]{1,0:T(8,128)(2,1)S(1)}, u32[]{:S(2)}, u32[]{:S(2)}) collective-permute-start(bf16[192,1024]{1,0:T(8,128)(2,1)} %get-tuple-element.16), channel_id=1, source_target_pairs={{0,2},{1,3},{2,0},{3,1},{4,6},{5,7},{6,4},{7,5},{8,10},{9,11},{10,... | collective-permute-start | bytes 1179656 | tf_op jit(solution)/shard_map/ppermute | solution.py:511
  58.7 13.1 %copy-start.4 = (f32[3,2,256]{2,1,0:T(2,128)S(1)}, f32[3,2,256]{2,1,0:T(2,128)}, u32[]{:S(2)}) copy-start(f32[3,2,256]{2,1,0:T(2,128)} %get-tuple-element.19) | copy-start | bytes 18436
  58.8 15.2 %collective-permute-start.4 = (bf16[192,1024]{1,0:T(8,128)(2,1)}, bf16[192,1024]{1,0:T(8,128)(2,1)S(1)}, u32[]{:S(2)}, u32[]{:S(2)}) collective-permute-start(bf16[192,1024]{1,0:T(8,128)(2,1)} %project.1), channel_id=1, source_target_pairs={{0,2},{1,3},{2,0},{3,1},{4,6},{5,7},{6,4},{7,5},{8,10},{9,11},{10,... | collective-permute-start | bytes 1179656 | tf_op jit(solution)/shard_map/ppermute | solution.py:513
  72.0 1.2 %collective-permute-start.5 = (f32[2,3,4,64]{3,1,0,2:T(4,128)S(1)}, f32[2,3,4,64]{3,1,0,2:T(4,128)S(1)}, u32[]{:S(2)}, u32[]{:S(2)}) collective-permute-start(f32[2,3,4,64]{3,1,0,2:T(4,128)S(1)} %get-tuple-element.23), channel_id=1, source_target_pairs={{0,1},{1,0},{2,3},{3,2},{4,5},{5,4},{6,7},{7,6},{8,9},{9,8},{10,11... | collective-permute-start | bytes 18440 | tf_op jit(solution)/shard_map/ppermute | solution.py:520
  74.0 1.1 %copy-start = (bf16[192,2048]{1,0:T(8,128)(2,1)S(1)}, bf16[192,2048]{1,0:T(8,128)(2,1)}, u32[]{:S(2)}) copy-start(bf16[192,2048]{1,0:T(8,128)(2,1)} %get-tuple-element.15.own_ref) | copy-start | bytes 2359300

commit v3 on v2

--- a/solution.py
+++ b/solution.py
@@ -18,105 +18,85 @@
 ON_CHIP = pl.BlockSpec(memory_space=VMEM)
 SCALARS = pl.BlockSpec(memory_space=pltpu.SMEM)
 VMEM_ALL = 60 * 1024 * 1024
-VMEM_MOST = 64600 * 1024
-
-
-def latent_kernel(tok_hbm, w_hbm, gain_hbm, out_ref, tok_v, w_v, gain_v, sems):
-    parts, tile, _ = tok_v.shape
-    copies = [pltpu.make_async_copy(w_hbm, w_v, sems.at[parts])]
-    for i in range(parts):
-        copies.append(pltpu.make_async_copy(tok_hbm.at[pl.ds(i * tile, tile)], tok_v.at[i], sems.at[i]))
-    copies.append(pltpu.make_async_copy(gain_hbm, gain_v, sems.at[parts + 1]))
-    for copy in copies:
-        copy.start()
-    copies[0].wait()
-    copies[-1].wait()
-    for i in range(parts):
-        copies[1 + i].wait()
-        projected = jnp.dot(tok_v[i], w_v[...], preferred_element_type=jnp.float32)
+VMEM_PART = 52 << 20
+
+
+def latent_kernel(tok_ref, w_ref, gain_ref, out_ref):
+    tile = math.gcd(tok_ref.shape[0], 256)
+    for at in range(0, tok_ref.shape[0], tile):
+        projected = jnp.dot(tok_ref[at : at + tile, :], w_ref[...], preferred_element_type=jnp.float32)
         inv_rms = lax.rsqrt(jnp.mean(projected * projected, axis=-1, keepdims=True) + epsilon)
-        out = projected * inv_rms * gain_v[...]
-        out_ref[i * tile : (i + 1) * tile, :] = out.astype(out_ref.dtype)
+        out = projected * inv_rms * gain_ref[...]
+        out_ref[at : at + tile, :] = out.astype(out_ref.dtype)
 
 
 def latents_of(tokens, w_latent, latent_gain):
     rows, width = tokens.shape
     rank = w_latent.shape[1]
-    tile = math.gcd(rows, 256)
     return pl.pallas_call(
         latent_kernel,
-        in_specs=[ANY, ANY, ANY],
+        in_specs=[ON_CHIP] * 3,
         out_specs=ON_CHIP,
         out_shape=jax.ShapeDtypeStruct((rows, rank), jnp.bfloat16),
-        scratch_shapes=[
-            VMEM((rows // tile, tile, width), jnp.bfloat16),
-            VMEM((width, rank), jnp.bfloat16),
-            VMEM((1, rank), jnp.float32),
-            DMA((rows // tile + 2,)),
-        ],
         cost_estimate=pl.CostEstimate(
             flops=2 * rows * width * rank, bytes_accessed=2 * rows * width, transcendentals=rows
         ),
-        compiler_params=pltpu.CompilerParams(vmem_limit_bytes=VMEM_MOST),
+        compiler_params=pltpu.CompilerParams(vmem_limit_bytes=12 << 20),
         name="latents",
     )(tokens, w_latent, latent_gain.reshape(1, rank))
 
 
-def query_kernel(tok_hbm, wa_hbm, wb_hbm, oa_hbm, ob_hbm, tok_v, w_v, o_v, tok_sem, w_sem, o_sem):
-    m, tile, _ = tok_v.shape
-    tiles = w_v.shape[0] // 2
-    step = w_v.shape[2]
+def query_kernel(tok_hbm, w_hbm, keep_hbm, give_hbm, tok_v, w_v, o_v, tok_sem, w_sem, o_sem):
+    _, m, tile, _ = tok_v.shape
+    tiles, _, step = w_v.shape
     core = lax.rem(lax.axis_index("tp"), 2)
     toks = [
-        pltpu.make_async_copy(tok_hbm.at[i, core], tok_v.at[i], tok_sem.at[i]) for i in range(m)
+        pltpu.make_async_copy(tok_hbm.at[i, lax.rem(core + 1 - side, 2)], tok_v.at[side, i], tok_sem.at[side, i])
+        for side in range(2)
+        for i in range(m)
     ]
     loads = [
-        pltpu.make_async_copy(
-            w_hbm.at[:, pl.ds(n * step, step)], w_v.at[u * tiles + n], w_sem.at[u * tiles + n]
-        )
-        for u, w_hbm in enumerate((wa_hbm, wb_hbm))
+        pltpu.make_async_copy(w_hbm.at[:, pl.ds(n * step, step)], w_v.at[n], w_sem.at[n])
         for n in range(tiles)
     ]
-    stores = [
-        pltpu.make_async_copy(
-            o_v.at[u * tiles + n], o_hbm.at[:, pl.ds(n * step, step)], o_sem.at[u * tiles + n]
-        )
-        for u, o_hbm in enumerate((oa_hbm, ob_hbm))
-        for n in range(tiles)
-    ]
-    for copy in toks + loads[:2]:
+    for copy in toks[:m] + loads + toks[m:]:
         copy.start()
-    for n in range(2 * tiles):
-        if n + 2 < 2 * tiles:
-            loads[n + 2].start()
-        loads[n].wait()
-        for i in range(m):
-            if n == 0:
-                toks[i].wait()
-            out = jnp.dot(tok_v[i], w_v[n], preferred_element_type=jnp.float32)
-            o_v[n, i * tile : (i + 1) * tile, :] = out.astype(o_v.dtype)
-        stores[n].start()
+    stores = []
+    for side, o_hbm in enumerate((give_hbm, keep_hbm)):
+        for copy in toks[side * m : side * m + m]:
+            copy.wait()
+        for n in range(tiles):
+            if side == 0:
+                loads[n].wait()
+            for i in range(m):
+                out = jnp.dot(tok_v[side, i], w_v[n], preferred_element_type=jnp.float32)
+                o_v[side, n, i * tile : (i + 1) * tile, :] = out.astype(o_v.dtype)
+            store = pltpu.make_async_copy(
+                o_v.at[side, n], o_hbm.at[:, pl.ds(n * step, step)], o_sem.at[side, n]
+            )
+            store.start()
+            stores.append(store)
     for copy in stores:
         copy.wait()
 
 
-def queries_of(tokens4, wq_a, wq_b):
+def queries_of(tokens4, w_query):
     m, _, tile, width = tokens4.shape
-    cols = wq_a.shape[1]
+    cols = w_query.shape[1]
     step = math.gcd(cols, 512)
     tiles = cols // step
     shape = jax.ShapeDtypeStruct((m * tile, cols), jnp.bfloat16)
     return pl.pallas_call(
         query_kernel,
-        in_specs=[ANY, ANY, ANY],
+        in_specs=[ANY, ANY],
         out_specs=[ANY, ANY],
         scratch_shapes=[
-            VMEM((m, tile, width), jnp.bfloat16),
-            VMEM((2 * tiles, width, step), jnp.bfloat16),
-            VMEM((2 * tiles, m * tile, step), jnp.bfloat16),
-            DMA((m,)),
-            DMA((2 * tiles,)),
-            DMA((2 * tiles,)),
+            VMEM((2, m, tile, width), jnp.bfloat16),
+            VMEM((tiles, width, step), jnp.bfloat16),
+            VMEM((2, tiles, m * tile, step), jnp.bfloat16),
+            DMA((2, m)),
+            DMA((tiles,)),
+            DMA((2, tiles)),
         ],
         out_shape=[shape, shape],
         cost_estimate=pl.CostEstimate(
@@ -126,7 +106,7 @@
         ),
         compiler_params=pltpu.CompilerParams(vmem_limit_bytes=VMEM_ALL),
         name="queries",
-    )(tokens4, wq_a, wq_b)
+    )(tokens4, w_query)
 
 
 def pick_kernel(asked_ref, lat_ref, out_ref):
@@ -148,7 +128,7 @@
         in_specs=[SCALARS, ON_CHIP],
         out_specs=ON_CHIP,
         out_shape=jax.ShapeDtypeStruct((owners, count, half, rank), latent4.dtype),
-        compiler_params=pltpu.CompilerParams(vmem_limit_bytes=VMEM_MOST),
+        compiler_params=pltpu.CompilerParams(vmem_limit_bytes=4 << 20),
         name="pick",
     )(asked, latent4)
 
@@ -216,7 +196,7 @@
         cost_estimate=pl.CostEstimate(
             flops=4 * rows * cols * width, bytes_accessed=4 * cols * width, transcendentals=0
         ),
-        compiler_params=pltpu.CompilerParams(vmem_limit_bytes=VMEM_ALL),
+        compiler_params=pltpu.CompilerParams(vmem_limit_bytes=VMEM_PART),
         name="project",
     )(ho, wo_a, wo_b)
 
@@ -333,61 +313,80 @@
     for k in range(0, key_len, chunk):
         val_v[:, k : k + chunk] = key_v[k : k + chunk, :].T
 
-    def scores(b, u, s_ref):
-        here = first + b
-        q = jnp.concatenate(
+    def queries(b, u):
+        return jnp.concatenate(
             [q_v[u, b, :, h * rank : (h + 1) * rank] for h in range(heads)], axis=0
         )
-        peak = jnp.full((8, unit), NEG, jnp.float32)
-        for at in range(0, key_len, chunk):
-            s = lax.dot_general(
-                key_v[at : at + chunk, :], q, (((1,), (1,)), ((), ())), preferred_element_type=jnp.float32
-            )
-            for k in range(0, chunk, half):
-                col = at + k
-                row = s[k : k + half]
-                if col < own_len:
-                    add = bl_ref[b, col : col + half, :]
-                    row = row + jnp.concatenate([add] * (unit // lanes), axis=1)
-                else:
-                    row = row + named_ref[here, own_blocks + (col - own_len) // half % slots]
-                s_ref[col : col + half, :] = row
-                for r in range(0, half, 8):
-                    peak = jnp.maximum(peak, row[r : r + 8])
-        return jnp.max(peak, axis=0, keepdims=True)
-
-    def weigh(b, u, s_ref, p_ref, peak):
-        mass = jnp.zeros((8, unit), jnp.float32)
-        for k in range(0, key_len, half):
+
+    def scores(at, b, q, s_ref, peak):
+        here = first + b
+        s = lax.dot_general(
+            key_v[at : at + chunk, :], q, (((1,), (1,)), ((), ())), preferred_element_type=jnp.float32
+        )
+        for k in range(0, chunk, half):
+            col = at + k
+            row = s[k : k + half]
+            if col < own_len:
+                add = bl_ref[b, col : col + half, :]
+                row = row + jnp.concatenate([add] * (unit // lanes), axis=1)
+            else:
+                row = row + named_ref[here, own_blocks + (col - own_len) // half % slots]
+            s_ref[col : col + half, :] = row
+            for r in range(0, half, 8):
+                peak = jnp.maximum(peak, row[r : r + 8])
+        return peak
+
+    def weigh(at, s_ref, p_ref, peak, mass):
+        for k in range(at, at + chunk, half):
             raised = jnp.exp2((s_ref[k : k + half, :] - peak) * exp_scale)
             p_ref[k : k + half, :] = raised.astype(p_ref.dtype)
             for r in range(0, half, 8):
                 mass = mass + raised[r : r + 8]
-        mass = jnp.sum(mass, axis=0, keepdims=True)
-        lse_ref[b, u : u + 1, :] = peak * scale + jnp.log(mass)
-        return 1.0 / mass
-
-    def gather(b, u, p_ref, inverse):
-        out = jnp.dot(val_v[...], p_ref[...], preferred_element_type=jnp.float32)
+        return mass
+
+    def place(b, u, out, inverse):
         out = (out * inverse).astype(ho_ref.dtype).T
         at = pl.multiple_of(b * blk_len, blk_len)
         for h in range(heads):
             ho_ref[u, pl.ds(at, blk_len), h * rank : (h + 1) * rank] = out[h * blk_len : (h + 1) * blk_len]
 
+    low = jnp.full((8, unit), NEG, jnp.float32)
+    top = lambda peak: jnp.max(peak, axis=0, keepdims=True)
+
+    def stage(score, weight, gather):
+        b, u, s_ref = score
+        q = queries(b, u)
+        next_peak = low
+        b1, u1, s1, p1, peak = weight
+        mass = jnp.zeros((8, unit), jnp.float32)
+        b2, u2, p2, inverse = gather
+        out = jnp.zeros((rank, unit), jnp.float32)
+        for at in range(0, key_len, chunk):
+            out = out + jnp.dot(
+                val_v[:, at : at + chunk], p2[at : at + chunk, :], preferred_element_type=jnp.float32
+            )
+            mass = weigh(at, s1, p1, peak, mass)
+            next_peak = scores(at, b, q, s_ref, next_peak)
+        place(b2, u2, out, inverse)
+        mass = jnp.sum(mass, axis=0, keepdims=True)
+        lse_ref[b1, u1 : u1 + 1, :] = peak * scale + jnp.log(mass)
+        return top(next_peak), 1.0 / mass
+
     def block(b, carry):
-        peak0, inverse1 = carry
-        peak1 = scores(b, 1, s1_ref)
-        inverse0 = weigh(b, 0, s0_ref, p0_ref, peak0)
-        gather(jnp.maximum(b - 1, 0), 1, p1_ref, inverse1)
-        after = scores(jnp.minimum(b + 1, count - 1), 0, s0_ref)
-        inverse1 = weigh(b, 1, s1_ref, p1_ref, peak1)
-        gather(b, 0, p0_ref, inverse0)
-        return after, inverse1
+        peak, inverse = carry
+        before = jnp.maximum(b - 1, 0)
+        after = jnp.minimum(b + 1, count - 1)
+        peak, inverse = stage((b, 1, s1_ref), (b, 0, s0_ref, p0_ref, peak), (before, 1, p1_ref, inverse))
+        return stage((after, 0, s0_ref), (b, 1, s1_ref, p1_ref, peak), (b, 0, p0_ref, inverse))
 
     p1_ref[...] = jnp.zeros_like(p1_ref)
-    start = (scores(0, 0, s0_ref), jnp.ones((1, unit), jnp.float32))
+    q0 = queries(0, 0)
+    peak0 = low
+    for at in range(0, key_len, chunk):
+        peak0 = scores(at, 0, q0, s0_ref, peak0)
+    start = (top(peak0), jnp.ones((1, unit), jnp.float32))
     _, inverse1 = lax.fori_loop(0, count, block, start)
-    gather(count - 1, 1, p1_ref, inverse1)
+    place(count - 1, 1, jnp.dot(val_v[...], p1_ref[...], preferred_element_type=jnp.float32), inverse1)
     keeps = [
         pltpu.make_async_copy(ho_ref, ho_hbm, ho_sem.at[0]),
         pltpu.make_async_copy(lse_ref, lse_hbm, ho_sem.at[1]),
@@ -440,7 +439,7 @@
             bytes_accessed=2 * key_len * rank + 4 * cols * width,
             transcendentals=2 * count * unit * key_len,
         ),
-        compiler_params=pltpu.CompilerParams(vmem_limit_bytes=VMEM_ALL),
+        compiler_params=pltpu.CompilerParams(vmem_limit_bytes=VMEM_PART),
         name="attend",
     )(named, qa, qb, latent, r1, r2, wo_a, wo_b)
 
@@ -462,7 +461,6 @@
     chip, core = tp // 2, tp % 2
     swap = [(i, i ^ 1) for i in range(n_tp)]
 
-    wq_other = lax.ppermute(w_query, "tp", swap)
 
     flat = chosen.reshape(1, per_device * picks)
     first_id = (jnp.arange(devices, dtype=jnp.int32) * per_device)[:, None]
@@ -483,7 +481,8 @@
     )
     r1 = fetched.reshape(devices * CAP * half, rank)
     r2 = lax.ppermute(r1, "tp", swap)
-    qa, qb = queries_of(tokens4, w_query, wq_other)
+    qa, give = queries_of(tokens4, w_query)
+    qb = lax.ppermute(give, "tp", swap)
 
     earlier = jnp.arange(devices, dtype=jnp.int32) < mine
     slots = jnp.stack(
@@ -500,7 +499,8 @@
 
     def work(k, cols):
         out, ho, lse = attend(named, qa4, qb4, latent, r1, r2, w_output, wo_other, cols, k, scale)
-        return out, ho, lse.reshape(tile_blocks, 2, heads, blk_len)
+        theirs = lax.ppermute(lse[:, 1], "tp", swap)
+        return out, ho, (lse[:, 0], theirs)
 
     lse_tiles = [None] * m
     arrived = []
@@ -515,14 +515,14 @@
     total, _, lse_tiles[0] = work(0, width)
     attended = finish(total, sum(arrived, []))
 
-    lse = jnp.stack(lse_tiles)
-    lse = lax.dynamic_slice_in_dim(jnp.concatenate([lse, lse], axis=0), (m - chip) % m, m, 0)
-    theirs = lax.ppermute(lse[:, :, 1], "tp", swap)
-    ours = lse[:, :, 0]
-    log_total = jnp.where(
-        core == 0, jnp.stack([ours, theirs], axis=1), jnp.stack([theirs, ours], axis=1)
-    )
-    log_total = jnp.swapaxes(log_total, 3, 4).reshape(tok_rows, heads)
+    tiles = []
+    for c in range(m):
+        for side in range(2):
+            at = [lax.rem(c - chip + m, m) == k for k in range(m)]
+            ours, theirs = (sum(jnp.where(at[k], lse_tiles[k][i], 0.0) for k in range(m)) for i in range(2))
+            tiles.append(jnp.where(core == side, ours, theirs))
+    log_total = jnp.stack(tiles).reshape(n_tp * tile_blocks, heads, blk_len)
+    log_total = jnp.swapaxes(log_total, 1, 2).reshape(tok_rows, heads)
     return (attended, log_total)
 
 

time: 76.7 us -> 73.2 us (0.954)
  Pallas kernels: 40.9 us -> 33.1 us
  local copies, waits for them, and re-layouts: 4.91 us -> 7.53 us
  waiting for transfers between devices: 14.7 us -> 16.3 us
    pallas_call x2, Pallas kernels: 12.9 us -> 7.68 us  [the longest x1 6.62 us: queries_of(): pl.pallas_call(query_kernel, in_specs=[ANY, ANY], out_specs=[ANY, ANY], s...]
    unnamed x12 -> x13, local copies, waits for them, and re-layouts: 2.42 us -> 5.82 us
    pallas_call x2, Pallas kernels: 21.2 us -> 19.8 us  [attend(): pl.pallas_call(functools.partial(attend_kernel, scale, ahead), in_specs=[...]
    ppermute x1, waiting for transfers between devices: 0.01 us -> 1.38 us  [layer(): r2 = lax.ppermute(r1, 'tp', swap)]
    another operation x5 -> x0, local copies, waits for them, and re-layouts: 0.89 us -> none  [the longest x4 0.88 us: layer(): lse = jnp.stack(lse_tiles)]
    pallas_call x1, Pallas kernels: 4.03 us -> 3.24 us  [project(): pl.pallas_call(project_kernel, in_specs=[ANY] * 3, out_specs=ANY, scratch...]
  transfers between devices with their start and end apart: 8 -> 9, of which waited for: 3 -> 4; matrix products, arithmetic and copies ran while one was open for 5% -> 3% of each run, Pallas kernels for 40% -> 30%
where the time goes in v3:
time: 73.2 us; the launch traced here: 72.7 us
  Pallas kernels  33.1 us (45%)
  waiting for transfers between devices  16.3 us (22%)
  starting transfers between devices  14.3 us (20%)
  local copies, waits for them, and re-layouts  7.53 us (10%)
  between operations  0.93 us (1%)
    pallas_call x2, Pallas kernels, attend(): pl.pallas_call(functools.partial(attend_kernel, scale, ahead), in_specs=[...  19.8 us
    all_to_all x1, waiting for transfers between devices, layer(): lax.all_to_all(reply, 'kv', split_axis=0, concat_axis=0, tiled=True)  7.7 us
    all_to_all x1, starting transfers between devices, layer(): lax.all_to_all(request, 'kv', split_axis=0, concat_axis=0, tiled=True)  7.32 us
    pallas_call x1, Pallas kernels, queries_of(): pl.pallas_call(query_kernel, in_specs=[ANY, ANY], out_specs=[ANY, ANY], s...  6.62 us
    all_to_all x1, waiting for transfers between devices, layer(): lax.all_to_all(request, 'kv', split_axis=0, concat_axis=0, tiled=True)  6.42 us
    unnamed x13, local copies, waits for them, and re-layouts  5.82 us
    all_to_all x1, starting transfers between devices, layer(): lax.all_to_all(reply, 'kv', split_axis=0, concat_axis=0, tiled=True)  3.59 us
    pallas_call x1, Pallas kernels, project(): pl.pallas_call(project_kernel, in_specs=[ANY] * 3, out_specs=ANY, scratch...  3.24 us
  transfers between devices with their start and end apart: 9, of which 4 were waited for; matrix products, arithmetic and copies ran while one was open for 3% of the time, Pallas kernels for 30%

profile of v3, /device:TPU:0, one launch (start us, length us, event | category | flops | bytes accessed | tf_op | source)
XLA Modules:
  0.0 72.7 jit_solution(4963517750732611459)
XLA Ops:
  0.6 0.0 copy-start
  0.6 1.9 %copy-done = bf16[768,2048]{1,0:T(8,128)(2,1)S(1)} copy-done((bf16[768,2048]{1,0:T(8,128)(2,1)S(1)}, bf16[768,2048]{1,0:T(8,128)(2,1)}, u32[]{:S(2)}) %copy-start) | copy-done | bytes 3145752
  2.5 0.0 copy-start.1
  2.5 1.2 %copy-done.1 = bf16[2048,256]{1,0:T(8,128)(2,1)S(1)} copy-done((bf16[2048,256]{1,0:T(8,128)(2,1)S(1)}, bf16[2048,256]{1,0:T(8,128)(2,1)}, u32[]{:S(2)}) %copy-start.1) | copy-done | bytes 1048600
  3.7 0.0 copy-start.3
  3.8 0.7 copy-done.3
  4.4 1.1 %latents.1.own_hbm = bf16[768,256]{1,0:T(8,128)(2,1)S(1)} custom-call(bf16[768,2048]{1,0:T(8,128)(2,1)S(1)} %copy-done, bf16[2048,256]{1,0:T(8,128)(2,1)S(1)} %copy-done.1, f32[1,256]{1,0:T(1,128)S(1)} %bitcast.48), custom_call_target="tpu_custom_call" | custom-call | flops 805306368 | bytes 3145728 | tf_op jit(solution)/shard_map/latents/pallas_call | solution.py:36
  5.5 0.6 collective-permute-start.2
  6.1 0.0 copy-start.4
  6.1 6.6 %queries.1 = (bf16[384,1024]{1,0:T(8,128)(2,1)}, bf16[384,1024]{1,0:T(8,128)(2,1)}) custom-call(bf16[2,2,192,2048]{3,2,1,0:T(8,128)(2,1)} %bitcast.43, bf16[2048,1024]{1,0:T(8,128)(2,1)} %w_hbm.1), custom_call_target="tpu_custom_call" | custom-call | flops 3221225472 | bytes 8388608 | tf_op jit(solution)/shard_map/queries/pallas_call | solution.py:89
  12.7 0.1 collective-permute-start
  12.8 0.0 copy-done.4
  12.8 0.1 ge.15
  12.9 0.2 select_reduce_fusion.1
  13.1 0.7 copy.21
  13.8 7.3 %all-to-all-start = ((s32[8,1,2]{2,1,0:T(1,128)}), s32[8,1,2]{2,1,0:T(1,128)S(1)}, u32[]{:S(2)}, u32[]{:S(2)}) async-start(s32[8,1,2]{2,1,0:T(1,128)} %copy.21), calls=%async_computation | async-start | bytes 8192 | tf_op jit(solution)/shard_map/all_to_all | solution.py:471
  21.1 6.4 %all-to-all-done.asked_ref = s32[8,1,2]{2,1,0:T(1,128)S(1)} async-done(((s32[8,1,2]{2,1,0:T(1,128)}), s32[8,1,2]{2,1,0:T(1,128)S(1)}, u32[]{:S(2)}, u32[]{:S(2)}) %all-to-all-start) | async-done | bytes 96 | tf_op jit(solution)/shard_map/all_to_all | solution.py:471
  27.5 1.4 %pick.1 = bf16[8,2,32,256]{3,2,1,0:T(8,128)(2,1)} custom-call(s32[8,1,2]{2,1,0:T(1,128)S(1)} %all-to-all-done.asked_ref, bf16[12,2,32,256]{3,2,1,0:T(8,128)(2,1)S(1)} %bitcast.44), custom_call_target="tpu_custom_call" | custom-call | tf_op jit(solution)/shard_map/pick/pallas_call | solution.py:126
  28.9 3.6 %all-to-all-start.1 = ((bf16[8,2,32,256]{3,2,1,0:T(8,128)(2,1)}), bf16[8,2,32,256]{3,2,1,0:T(8,128)(2,1)S(1)}, u32[]{:S(2)}, u32[]{:S(2)}) async-start(bf16[8,2,32,256]{3,2,1,0:T(8,128)(2,1)} %pick.1), calls=%async_computation.1 | async-start | bytes 524288 | tf_op jit(solution)/shard_map/all_to_all | solution.py:479
  32.5 0.1 copy.20
  32.6 0.1 reshape.89
  32.7 0.1 pad_add_fusion.1
  32.7 7.7 %all-to-all-done.1 = bf16[8,2,32,256]{3,2,1,0:T(8,128)(2,1)S(1)} async-done(((bf16[8,2,32,256]{3,2,1,0:T(8,128)(2,1)}), bf16[8,2,32,256]{3,2,1,0:T(8,128)(2,1)S(1)}, u32[]{:S(2)}, u32[]{:S(2)}) %all-to-all-start.1) | async-done | bytes 262176 | tf_op jit(solution)/shard_map/all_to_all | solution.py:479
  40.5 0.0 collective-permute-start.1
  40.5 0.1 compare_reduce_fusion
  40.6 1.4 %collective-permute-done.1.r2_hbm = bf16[512,256]{1,0:T(8,128)(2,1)S(1)} collective-permute-done((bf16[512,256]{1,0:T(8,128)(2,1)S(1)}, bf16[512,256]{1,0:T(8,128)(2,1)S(1)}, u32[]{:S(2)}, u32[]{:S(2)}) %collective-permute-start.1) | collective-permute-done | bytes 262176 | tf_op jit(solution)/shard_map/ppermute | solution.py:483
  42.0 0.0 collective-permute-done
  42.0 0.0 copy-start.5
  42.0 0.0 collective-permute-done.2.wb_hbm
  42.0 0.9 %copy-done.5 = bf16[384,1024]{1,0:T(8,128)(2,1)} copy-done((bf16[384,1024]{1,0:T(8,128)(2,1)}, bf16[384,1024]{1,0:T(8,128)(2,1)S(1)}, u32[]{:S(2)}) %copy-start.5) | copy-done | bytes 786456
  42.9 8.9 %attend.3 = (bf16[192,1024]{1,0:T(8,128)(2,1)S(1)}, bf16[2,192,1024]{2,1,0:T(8,128)(2,1)}, f32[3,2,256]{2,1,0:T(2,128)S(1)}) custom-call(f32[12,28]{1,0:T(8,128)S(1)} %broadcast_select_fusion.named_hbm, bf16[2,3,64,1024]{3,2,1,0:T(8,128)(2,1)} %bitcast.55, bf16[2,3,64,1024]{3,2,1,0:T(8,128)(2,1)} %bitcast.53, bf16[768,256]{1,0:T(8,128)(2,1)S(1)} %latents.1.own_hbm, ...), custom_call_target="tpu_custom_call" | custom-call | flops 3623878656 | bytes 5111808 | tf_op jit(solution)/shard_map/attend/pallas_call | solution.py:409
  51.8 1.5 %collective-permute-start.3 = (bf16[192,1024]{1,0:T(8,128)(2,1)S(1)}, bf16[192,1024]{1,0:T(8,128)(2,1)S(1)}, u32[]{:S(2)}, u32[]{:S(2)}) collective-permute-start(bf16[192,1024]{1,0:T(8,128)(2,1)S(1)} %get-tuple-element.16), channel_id=1, source_target_pairs={{0,2},{1,3},{2,0},{3,1},{4,6},{5,7},{6,4},{7,5},{8,10},{9,11},{10,... | collective-permute-start | bytes 1179656 | tf_op jit(solution)/shard_map/ppermute | solution.py:511
  53.3 0.0 copy-start.2
  53.3 1.1 %copy-done.2 = bf16[2,192,1024]{2,1,0:T(8,128)(2,1)S(1)} copy-done((bf16[2,192,1024]{2,1,0:T(8,128)(2,1)S(1)}, bf16[2,192,1024]{2,1,0:T(8,128)(2,1)}, u32[]{:S(2)}) %copy-start.2) | copy-done | bytes 786456
  54.5 3.2 %project.1 = bf16[192,1024]{1,0:T(8,128)(2,1)S(1)} custom-call(bf16[2,192,1024]{2,1,0:T(8,128)(2,1)S(1)} %copy-done.2, bf16[1024,2048]{1,0:T(8,128)(2,1)} %wa_hbm.5, bf16[1024,2048]{1,0:T(8,128)(2,1)} %collective-permute-done.2.wb_hbm), custom_call_target="tpu_custom_call" | custom-call | flops 805306368 | bytes 4194304 | tf_op jit(solution)/shard_map/project/pallas_call | solution.py:183
  57.7 0.6 collective-permute-start.4
  58.3 0.1 collective-permute-start.6
  58.4 10.9 %attend.2 = (bf16[192,2048]{1,0:T(8,128)(2,1)S(1)}, bf16[2,192,1024]{2,1,0:T(8,128)(2,1)}, f32[3,2,256]{2,1,0:T(2,128)S(1)}) custom-call(f32[12,28]{1,0:T(8,128)S(1)} %broadcast_select_fusion.named_hbm, bf16[2,3,64,1024]{3,2,1,0:T(8,128)(2,1)} %bitcast.56, bf16[2,3,64,1024]{3,2,1,0:T(8,128)(2,1)} %bitcast.54, bf16[768,256]{1,0:T(8,128)(2,1)S(1)} %latents.1.own_hbm, ...), custom_call_target="tpu_custom_call" | custom-call | flops 4429185024 | bytes 9306112 | tf_op jit(solution)/shard_map/attend/pallas_call | solution.py:409
  69.4 0.5 collective-permute-start.5
  69.9 0.0 collective-permute-done.6
  69.9 0.8 %collective-permute-done.5 = f32[3,256]{1,0:T(4,128)S(1)} collective-permute-done((f32[3,256]{1,0:T(4,128)S(1)}, f32[3,256]{1,0:T(4,128)S(1)}, u32[]{:S(2)}, u32[]{:S(2)}) %collective-permute-start.5) | collective-permute-done | bytes 3104 | tf_op jit(solution)/shard_map/ppermute | solution.py:502
  70.8 0.1 reshape.96
  70.9 0.7 reshape.97
  71.5 0.0 collective-permute-done.3.refs_0_
  71.6 0.0 collective-permute-done.4.refs_1_
  71.6 1.0 %finish.1 = bf16[192,2048]{1,0:T(8,128)(2,1)} custom-call(bf16[192,2048]{1,0:T(8,128)(2,1)S(1)} %get-tuple-element.15.own_ref, bf16[192,1024]{1,0:T(8,128)(2,1)S(1)} %collective-permute-done.3.refs_0_, bf16[192,1024]{1,0:T(8,128)(2,1)S(1)} %collective-permute-done.4.refs_1_), custom_call_target="tpu_custom_call" | custom-call | tf_op jit(solution)/shard_map/finish/pallas_call | solution.py:224
  (14 shorter events, 0.1 us)
Async XLA Ops:
  0.6 1.9 %copy-start = (bf16[768,2048]{1,0:T(8,128)(2,1)S(1)}, bf16[768,2048]{1,0:T(8,128)(2,1)}, u32[]{:S(2)}) copy-start(bf16[768,2048]{1,0:T(8,128)(2,1)} %tok_ref.1) | copy-start | bytes 9437188
  2.5 1.2 %copy-start.1 = (bf16[2048,256]{1,0:T(8,128)(2,1)S(1)}, bf16[2048,256]{1,0:T(8,128)(2,1)}, u32[]{:S(2)}) copy-start(bf16[2048,256]{1,0:T(8,128)(2,1)} %w_ref.1) | copy-start | bytes 3145732
  3.7 0.7 copy-start.3
  5.5 36.5 %collective-permute-start.2 = (bf16[1024,2048]{1,0:T(8,128)(2,1)}, bf16[1024,2048]{1,0:T(8,128)(2,1)}, u32[]{:S(2)}, u32[]{:S(2)}) collective-permute-start(bf16[1024,2048]{1,0:T(8,128)(2,1)} %wa_hbm.5), channel_id=1, source_target_pairs={{0,1},{1,0},{2,3},{3,2},{4,5},{5,4},{6,7},{7,6},{8,9},{9,8},{10,11... | collective-permute-start | bytes 12582920 | tf_op jit(solution)/shard_map/ppermute | solution.py:475
  6.1 6.7 %copy-start.4 = (s32[12,32]{1,0:T(8,128)S(1)}, s32[12,32]{1,0:T(8,128)}, u32[]{:S(2)}) copy-start(s32[12,32]{1,0:T(8,128)} %param.11) | copy-start | bytes 4612
  12.7 29.3 %collective-permute-start = (bf16[384,1024]{1,0:T(8,128)(2,1)}, bf16[384,1024]{1,0:T(8,128)(2,1)S(1)}, u32[]{:S(2)}, u32[]{:S(2)}) collective-permute-start(bf16[384,1024]{1,0:T(8,128)(2,1)} %get-tuple-element.12), channel_id=1, source_target_pairs={{0,1},{1,0},{2,3},{3,2},{4,5},{5,4},{6,7},{7,6},{8,9},{9,8},{10,11... | collective-permute-start | bytes 2359304 | tf_op jit(solution)/shard_map/ppermute | solution.py:485
  13.8 13.7 %all-to-all-start = ((s32[8,1,2]{2,1,0:T(1,128)}), s32[8,1,2]{2,1,0:T(1,128)S(1)}, u32[]{:S(2)}, u32[]{:S(2)}) async-start(s32[8,1,2]{2,1,0:T(1,128)} %copy.21), calls=%async_computation | async-start | bytes 8192 | tf_op jit(solution)/shard_map/all_to_all | solution.py:471
  28.9 11.6 %all-to-all-start.1 = ((bf16[8,2,32,256]{3,2,1,0:T(8,128)(2,1)}), bf16[8,2,32,256]{3,2,1,0:T(8,128)(2,1)S(1)}, u32[]{:S(2)}, u32[]{:S(2)}) async-start(bf16[8,2,32,256]{3,2,1,0:T(8,128)(2,1)} %pick.1), calls=%async_computation.1 | async-start | bytes 524288 | tf_op jit(solution)/shard_map/all_to_all | solution.py:479
  40.5 1.5 %collective-permute-start.1 = (bf16[512,256]{1,0:T(8,128)(2,1)S(1)}, bf16[512,256]{1,0:T(8,128)(2,1)S(1)}, u32[]{:S(2)}, u32[]{:S(2)}) collective-permute-start(bf16[512,256]{1,0:T(8,128)(2,1)S(1)} %bitcast.45), channel_id=1, source_target_pairs={{0,1},{1,0},{2,3},{3,2},{4,5},{5,4},{6,7},{7,6},{8,9},{9,8},{10,11... | collective-permute-start | bytes 786440 | tf_op jit(solution)/shard_map/ppermute | solution.py:483
  42.0 0.9 %copy-start.5 = (bf16[384,1024]{1,0:T(8,128)(2,1)}, bf16[384,1024]{1,0:T(8,128)(2,1)S(1)}, u32[]{:S(2)}) copy-start(bf16[384,1024]{1,0:T(8,128)(2,1)S(1)} %collective-permute-done) | copy-start | bytes 2359300
  51.8 19.8 %collective-permute-start.3 = (bf16[192,1024]{1,0:T(8,128)(2,1)S(1)}, bf16[192,1024]{1,0:T(8,128)(2,1)S(1)}, u32[]{:S(2)}, u32[]{:S(2)}) collective-permute-start(bf16[192,1024]{1,0:T(8,128)(2,1)S(1)} %get-tuple-element.16), channel_id=1, source_target_pairs={{0,2},{1,3},{2,0},{3,1},{4,6},{5,7},{6,4},{7,5},{8,10},{9,11},{10,... | collective-permute-start | bytes 1179656 | tf_op jit(solution)/shard_map/ppermute | solution.py:511
  53.3 1.1 %copy-start.2 = (bf16[2,192,1024]{2,1,0:T(8,128)(2,1)S(1)}, bf16[2,192,1024]{2,1,0:T(8,128)(2,1)}, u32[]{:S(2)}) copy-start(bf16[2,192,1024]{2,1,0:T(8,128)(2,1)} %get-tuple-element.17.ho_hbm) | copy-start | bytes 2359300
  57.7 13.8 %collective-permute-start.4 = (bf16[192,1024]{1,0:T(8,128)(2,1)S(1)}, bf16[192,1024]{1,0:T(8,128)(2,1)S(1)}, u32[]{:S(2)}, u32[]{:S(2)}) collective-permute-start(bf16[192,1024]{1,0:T(8,128)(2,1)S(1)} %project.1), channel_id=1, source_target_pairs={{0,2},{1,3},{2,0},{3,1},{4,6},{5,7},{6,4},{7,5},{8,10},{9,11},{10,... | collective-permute-start | bytes 1179656 | tf_op jit(solution)/shard_map/ppermute | solution.py:513
  58.3 11.6 %collective-permute-start.6 = (f32[3,256]{1,0:T(4,128)S(1)}, f32[3,256]{1,0:T(4,128)S(1)}, u32[]{:S(2)}, u32[]{:S(2)}) collective-permute-start(f32[3,256]{1,0:T(4,128)S(1)} %bitcast.52), channel_id=1, source_target_pairs={{0,1},{1,0},{2,3},{3,2},{4,5},{5,4},{6,7},{7,6},{8,9},{9,8},{10,11... | collective-permute-start | bytes 9224 | tf_op jit(solution)/shard_map/ppermute | solution.py:502
  69.4 1.4 %collective-permute-start.5 = (f32[3,256]{1,0:T(4,128)S(1)}, f32[3,256]{1,0:T(4,128)S(1)}, u32[]{:S(2)}, u32[]{:S(2)}) collective-permute-start(f32[3,256]{1,0:T(4,128)S(1)} %slice_bitcast_fusion), channel_id=1, source_target_pairs={{0,1},{1,0},{2,3},{3,2},{4,5},{5,4},{6,7},{7,6},{8,9},{9,8},{10,11... | collective-permute-start | bytes 9224 | tf_op jit(solution)/shard_map/ppermute | solution.py:502

commit v4 on v3

--- a/solution.py
+++ b/solution.py
@@ -235,6 +235,7 @@
 def attend_kernel(
     scale,
     ahead,
+    groups,
     named_hbm,
     qa_hbm,
     qb_hbm,
@@ -273,7 +274,7 @@
     own_blocks = own_len // blk_len
     slots = rem_len // half
     lanes = bl_ref.shape[2]
-    unit = heads * blk_len
+    unit = 2 // groups * heads * blk_len
     exp_scale = scale * math.log2(math.e)
     tp = lax.axis_index("tp")
     chip = lax.rem(tp // 2 + ahead, qa_hbm.shape[0])
@@ -313,9 +314,16 @@
     for k in range(0, key_len, chunk):
         val_v[:, k : k + chunk] = key_v[k : k + chunk, :].T
 
-    def queries(b, u):
+    sides = 2 // groups
+
+    def queries(b, g):
         return jnp.concatenate(
-            [q_v[u, b, :, h * rank : (h + 1) * rank] for h in range(heads)], axis=0
+            [
+                q_v[u, b, :, h * rank : (h + 1) * rank]
+                for u in range(g * sides, (g + 1) * sides)
+                for h in range(heads)
+            ],
+            axis=0,
         )
 
     def scores(at, b, q, s_ref, peak):
@@ -344,49 +352,49 @@
                 mass = mass + raised[r : r + 8]
         return mass
 
-    def place(b, u, out, inverse):
+    def place(b, g, out, inverse):
         out = (out * inverse).astype(ho_ref.dtype).T
-        at = pl.multiple_of(b * blk_len, blk_len)
-        for h in range(heads):
-            ho_ref[u, pl.ds(at, blk_len), h * rank : (h + 1) * rank] = out[h * blk_len : (h + 1) * blk_len]
-
-    low = jnp.full((8, unit), NEG, jnp.float32)
-    top = lambda peak: jnp.max(peak, axis=0, keepdims=True)
-
-    def stage(score, weight, gather):
-        b, u, s_ref = score
-        q = queries(b, u)
-        next_peak = low
-        b1, u1, s1, p1, peak = weight
-        mass = jnp.zeros((8, unit), jnp.float32)
-        b2, u2, p2, inverse = gather
-        out = jnp.zeros((rank, unit), jnp.float32)
+        for i in range(sides * heads):
+            u, h = g * sides + i // heads, i % heads
+            ho_ref[u, b * blk_len : (b + 1) * blk_len, h * rank : (h + 1) * rank] = out[
+                i * blk_len : (i + 1) * blk_len
+            ]
+
+    units = [(b, g) for b in range(count) for g in range(groups)]
+    s_refs, p_refs = (s0_ref, s1_ref), (p0_ref, p1_ref)
+    peaks, inverses = {}, {}
+    for t in range(-1, len(units) + 1):
+        score, weight, gather = t + 1 < len(units), 0 <= t < len(units), t >= 1
+        if score:
+            q = queries(*units[t + 1])
+            peak = jnp.full((8, unit), NEG, jnp.float32)
+        if weight:
+            mass = jnp.zeros((8, unit), jnp.float32)
+        if gather:
+            out = jnp.zeros((rank, unit), jnp.float32)
         for at in range(0, key_len, chunk):
-            out = out + jnp.dot(
-                val_v[:, at : at + chunk], p2[at : at + chunk, :], preferred_element_type=jnp.float32
-            )
-            mass = weigh(at, s1, p1, peak, mass)
-            next_peak = scores(at, b, q, s_ref, next_peak)
-        place(b2, u2, out, inverse)
-        mass = jnp.sum(mass, axis=0, keepdims=True)
-        lse_ref[b1, u1 : u1 + 1, :] = peak * scale + jnp.log(mass)
-        return top(next_peak), 1.0 / mass
-
-    def block(b, carry):
-        peak, inverse = carry
-        before = jnp.maximum(b - 1, 0)
-        after = jnp.minimum(b + 1, count - 1)
-        peak, inverse = stage((b, 1, s1_ref), (b, 0, s0_ref, p0_ref, peak), (before, 1, p1_ref, inverse))
-        return stage((after, 0, s0_ref), (b, 1, s1_ref, p1_ref, peak), (b, 0, p0_ref, inverse))
-
-    p1_ref[...] = jnp.zeros_like(p1_ref)
-    q0 = queries(0, 0)
-    peak0 = low
-    for at in range(0, key_len, chunk):
-        peak0 = scores(at, 0, q0, s0_ref, peak0)
-    start = (top(peak0), jnp.ones((1, unit), jnp.float32))
-    _, inverse1 = lax.fori_loop(0, count, block, start)
-    place(count - 1, 1, jnp.dot(val_v[...], p1_ref[...], preferred_element_type=jnp.float32), inverse1)
+            if gather:
+                out = out + jnp.dot(
+                    val_v[:, at : at + chunk],
+                    p_refs[(t - 1) % 2][at : at + chunk, :],
+                    preferred_element_type=jnp.float32,
+                )
+            if weight:
+                mass = weigh(at, s_refs[t % 2], p_refs[t % 2], peaks[t], mass)
+            if score:
+                peak = scores(at, units[t + 1][0], q, s_refs[(t + 1) % 2], peak)
+        if gather:
+            place(*units[t - 1], out, inverses[t - 1])
+        if weight:
+            b, g = units[t]
+            mass = jnp.sum(mass, axis=0, keepdims=True)
+            inverses[t] = 1.0 / mass
+            total = peaks[t] * scale + jnp.log(mass)
+            for i in range(sides):
+                part = unit // sides
+                lse_ref[b, g * sides + i : g * sides + i + 1, :] = total[:, i * part : (i + 1) * part]
+        if score:
+            peaks[t + 1] = jnp.max(peak, axis=0, keepdims=True)
     keeps = [
         pltpu.make_async_copy(ho_ref, ho_hbm, ho_sem.at[0]),
         pltpu.make_async_copy(lse_ref, lse_hbm, ho_sem.at[1]),
@@ -403,11 +411,13 @@
     own_len, rank = latent.shape
     heads = cols // rank
     key_len = own_len + 2 * r1.shape[0]
-    step = math.gcd(width, 512)
+    step = math.gcd(width, 1024)
     tiles = width // step
-    unit = heads * blk_len
+    side = heads * blk_len
+    groups = 1 if key_len <= 4096 else 2
+    unit = 2 // groups * side
     return pl.pallas_call(
-        functools.partial(attend_kernel, scale, ahead),
+        functools.partial(attend_kernel, scale, ahead, groups),
         in_specs=[ANY] * 8,
         out_specs=[ANY] * 3,
         scratch_shapes=[
@@ -423,7 +433,7 @@
                 VMEM((key_len, unit), jnp.bfloat16),
                 VMEM((count, own_len, 2 * blk_len), jnp.float32),
                 VMEM((2, count * blk_len, cols), jnp.bfloat16),
-                VMEM((count, 2, unit), jnp.float32),
+                VMEM((count, 2, side), jnp.float32),
                 DMA((6,)),
                 DMA((tiles, 2)),
                 DMA((tiles,)),
@@ -432,12 +442,12 @@
         out_shape=[
             jax.ShapeDtypeStruct((count * blk_len, width), jnp.bfloat16),
             jax.ShapeDtypeStruct((2, count * blk_len, cols), jnp.bfloat16),
-            jax.ShapeDtypeStruct((count, 2, unit), jnp.float32),
+            jax.ShapeDtypeStruct((count, 2, side), jnp.float32),
         ],
         cost_estimate=pl.CostEstimate(
-            flops=8 * count * unit * key_len * rank + 4 * count * blk_len * cols * width,
+            flops=8 * count * side * key_len * rank + 4 * count * blk_len * cols * width,
             bytes_accessed=2 * key_len * rank + 4 * cols * width,
-            transcendentals=2 * count * unit * key_len,
+            transcendentals=2 * count * side * key_len,
         ),
         compiler_params=pltpu.CompilerParams(vmem_limit_bytes=VMEM_PART),
         name="attend",

time: 73.2 us -> 71.6 us (0.978)
  Pallas kernels: 33.1 us -> 29.6 us
  waiting for transfers between devices: 16.3 us -> 18.2 us
    pallas_call x2, Pallas kernels: 19.8 us -> 16.4 us  [attend(): pl.pallas_call(functools.partial(attend_kernel, scale, ahead, groups), in...]
    ppermute x1, waiting for transfers between devices: 0.01 us -> 1.89 us  [layer(): piece1 = lax.ppermute(out1, 'tp', to_chip)]
  transfers between devices with their start and end apart: 9 -> 9, of which waited for: 4 -> 5; matrix products, arithmetic and copies ran while one was open for 3% -> 3% of each run, Pallas kernels for 30% -> 28%
where the time goes in v4:
time: 71.6 us; the launch traced here: 71.1 us
  Pallas kernels  29.6 us (41%)
  waiting for transfers between devices  18.2 us (25%)
  starting transfers between devices  14.3 us (20%)
  local copies, waits for them, and re-layouts  7.53 us (11%)
  between operations  0.93 us (1%)
    pallas_call x2, Pallas kernels, attend(): pl.pallas_call(functools.partial(attend_kernel, scale, ahead, groups), in...  16.4 us
    all_to_all x1, waiting for transfers between devices, layer(): lax.all_to_all(reply, 'kv', split_axis=0, concat_axis=0, tiled=True)  7.7 us
    all_to_all x1, starting transfers between devices, layer(): lax.all_to_all(request, 'kv', split_axis=0, concat_axis=0, tiled=True)  7.32 us
    pallas_call x1, Pallas kernels, queries_of(): pl.pallas_call(query_kernel, in_specs=[ANY, ANY], out_specs=[ANY, ANY], s...  6.62 us
    all_to_all x1, waiting for transfers between devices, layer(): lax.all_to_all(request, 'kv', split_axis=0, concat_axis=0, tiled=True)  6.42 us
    unnamed x13, local copies, waits for them, and re-layouts  5.82 us
    all_to_all x1, starting transfers between devices, layer(): lax.all_to_all(reply, 'kv', split_axis=0, concat_axis=0, tiled=True)  3.59 us
    pallas_call x1, Pallas kernels, project(): pl.pallas_call(project_kernel, in_specs=[ANY] * 3, out_specs=ANY, scratch...  3.24 us
  transfers between devices with their start and end apart: 9, of which 5 were waited for; matrix products, arithmetic and copies ran while one was open for 3% of the time, Pallas kernels for 28%

profile of v4, /device:TPU:0, one launch (start us, length us, event | category | flops | bytes accessed | tf_op | source)
XLA Modules:
  0.0 71.1 jit_solution(8610434075499175394)
XLA Ops:
  0.6 0.0 copy-start
  0.6 1.9 %copy-done = bf16[768,2048]{1,0:T(8,128)(2,1)S(1)} copy-done((bf16[768,2048]{1,0:T(8,128)(2,1)S(1)}, bf16[768,2048]{1,0:T(8,128)(2,1)}, u32[]{:S(2)}) %copy-start) | copy-done | bytes 3145752
  2.5 0.0 copy-start.1
  2.5 1.2 %copy-done.1 = bf16[2048,256]{1,0:T(8,128)(2,1)S(1)} copy-done((bf16[2048,256]{1,0:T(8,128)(2,1)S(1)}, bf16[2048,256]{1,0:T(8,128)(2,1)}, u32[]{:S(2)}) %copy-start.1) | copy-done | bytes 1048600
  3.7 0.0 copy-start.3
  3.8 0.7 copy-done.3
  4.4 1.1 %latents.1.own_hbm = bf16[768,256]{1,0:T(8,128)(2,1)S(1)} custom-call(bf16[768,2048]{1,0:T(8,128)(2,1)S(1)} %copy-done, bf16[2048,256]{1,0:T(8,128)(2,1)S(1)} %copy-done.1, f32[1,256]{1,0:T(1,128)S(1)} %bitcast.48), custom_call_target="tpu_custom_call" | custom-call | flops 805306368 | bytes 3145728 | tf_op jit(solution)/shard_map/latents/pallas_call | solution.py:36
  5.5 0.6 collective-permute-start.2
  6.1 0.0 copy-start.4
  6.1 6.6 %queries.1 = (bf16[384,1024]{1,0:T(8,128)(2,1)}, bf16[384,1024]{1,0:T(8,128)(2,1)}) custom-call(bf16[2,2,192,2048]{3,2,1,0:T(8,128)(2,1)} %bitcast.43, bf16[2048,1024]{1,0:T(8,128)(2,1)} %w_hbm.1), custom_call_target="tpu_custom_call" | custom-call | flops 3221225472 | bytes 8388608 | tf_op jit(solution)/shard_map/queries/pallas_call | solution.py:89
  12.7 0.1 collective-permute-start
  12.8 0.0 copy-done.4
  12.8 0.1 ge.15
  12.9 0.2 select_reduce_fusion.1
  13.1 0.7 copy.21
  13.8 7.3 %all-to-all-start = ((s32[8,1,2]{2,1,0:T(1,128)}), s32[8,1,2]{2,1,0:T(1,128)S(1)}, u32[]{:S(2)}, u32[]{:S(2)}) async-start(s32[8,1,2]{2,1,0:T(1,128)} %copy.21), calls=%async_computation | async-start | bytes 8192 | tf_op jit(solution)/shard_map/all_to_all | solution.py:481
  21.1 6.4 %all-to-all-done.asked_ref = s32[8,1,2]{2,1,0:T(1,128)S(1)} async-done(((s32[8,1,2]{2,1,0:T(1,128)}), s32[8,1,2]{2,1,0:T(1,128)S(1)}, u32[]{:S(2)}, u32[]{:S(2)}) %all-to-all-start) | async-done | bytes 96 | tf_op jit(solution)/shard_map/all_to_all | solution.py:481
  27.5 1.4 %pick.1 = bf16[8,2,32,256]{3,2,1,0:T(8,128)(2,1)} custom-call(s32[8,1,2]{2,1,0:T(1,128)S(1)} %all-to-all-done.asked_ref, bf16[12,2,32,256]{3,2,1,0:T(8,128)(2,1)S(1)} %bitcast.44), custom_call_target="tpu_custom_call" | custom-call | tf_op jit(solution)/shard_map/pick/pallas_call | solution.py:126
  28.9 3.6 %all-to-all-start.1 = ((bf16[8,2,32,256]{3,2,1,0:T(8,128)(2,1)}), bf16[8,2,32,256]{3,2,1,0:T(8,128)(2,1)S(1)}, u32[]{:S(2)}, u32[]{:S(2)}) async-start(bf16[8,2,32,256]{3,2,1,0:T(8,128)(2,1)} %pick.1), calls=%async_computation.1 | async-start | bytes 524288 | tf_op jit(solution)/shard_map/all_to_all | solution.py:489
  32.5 0.1 copy.20
  32.6 0.1 reshape.89
  32.7 0.1 pad_add_fusion.1
  32.7 7.7 %all-to-all-done.1 = bf16[8,2,32,256]{3,2,1,0:T(8,128)(2,1)S(1)} async-done(((bf16[8,2,32,256]{3,2,1,0:T(8,128)(2,1)}), bf16[8,2,32,256]{3,2,1,0:T(8,128)(2,1)S(1)}, u32[]{:S(2)}, u32[]{:S(2)}) %all-to-all-start.1) | async-done | bytes 262176 | tf_op jit(solution)/shard_map/all_to_all | solution.py:489
  40.5 0.0 collective-permute-start.1
  40.5 0.1 compare_reduce_fusion
  40.6 1.4 %collective-permute-done.1.r2_hbm = bf16[512,256]{1,0:T(8,128)(2,1)S(1)} collective-permute-done((bf16[512,256]{1,0:T(8,128)(2,1)S(1)}, bf16[512,256]{1,0:T(8,128)(2,1)S(1)}, u32[]{:S(2)}, u32[]{:S(2)}) %collective-permute-start.1) | collective-permute-done | bytes 262176 | tf_op jit(solution)/shard_map/ppermute | solution.py:493
  42.0 0.0 collective-permute-done
  42.0 0.0 copy-start.5
  42.0 0.0 collective-permute-done.2.wb_hbm
  42.0 0.9 %copy-done.5 = bf16[384,1024]{1,0:T(8,128)(2,1)} copy-done((bf16[384,1024]{1,0:T(8,128)(2,1)}, bf16[384,1024]{1,0:T(8,128)(2,1)S(1)}, u32[]{:S(2)}) %copy-start.5) | copy-done | bytes 786456
  42.9 7.4 %attend.3 = (bf16[192,1024]{1,0:T(8,128)(2,1)S(1)}, bf16[2,192,1024]{2,1,0:T(8,128)(2,1)}, f32[3,2,256]{2,1,0:T(2,128)S(1)}) custom-call(f32[12,28]{1,0:T(8,128)S(1)} %broadcast_select_fusion.named_hbm, bf16[2,3,64,1024]{3,2,1,0:T(8,128)(2,1)} %bitcast.55, bf16[2,3,64,1024]{3,2,1,0:T(8,128)(2,1)} %bitcast.53, bf16[768,256]{1,0:T(8,128)(2,1)S(1)} %latents.1.own_hbm, ...), custom_call_target="tpu_custom_call" | custom-call | flops 3623878656 | bytes 5111808 | tf_op jit(solution)/shard_map/attend/pallas_call | solution.py:419
  50.3 1.5 %collective-permute-start.3 = (bf16[192,1024]{1,0:T(8,128)(2,1)S(1)}, bf16[192,1024]{1,0:T(8,128)(2,1)S(1)}, u32[]{:S(2)}, u32[]{:S(2)}) collective-permute-start(bf16[192,1024]{1,0:T(8,128)(2,1)S(1)} %get-tuple-element.16), channel_id=1, source_target_pairs={{0,2},{1,3},{2,0},{3,1},{4,6},{5,7},{6,4},{7,5},{8,10},{9,11},{10,... | collective-permute-start | bytes 1179656 | tf_op jit(solution)/shard_map/ppermute | solution.py:521
  51.9 0.0 copy-start.2
  51.9 1.1 %copy-done.2 = bf16[2,192,1024]{2,1,0:T(8,128)(2,1)S(1)} copy-done((bf16[2,192,1024]{2,1,0:T(8,128)(2,1)S(1)}, bf16[2,192,1024]{2,1,0:T(8,128)(2,1)}, u32[]{:S(2)}) %copy-start.2) | copy-done | bytes 786456
  53.0 3.2 %project.1 = bf16[192,1024]{1,0:T(8,128)(2,1)S(1)} custom-call(bf16[2,192,1024]{2,1,0:T(8,128)(2,1)S(1)} %copy-done.2, bf16[1024,2048]{1,0:T(8,128)(2,1)} %wa_hbm.5, bf16[1024,2048]{1,0:T(8,128)(2,1)} %collective-permute-done.2.wb_hbm), custom_call_target="tpu_custom_call" | custom-call | flops 805306368 | bytes 4194304 | tf_op jit(solution)/shard_map/project/pallas_call | solution.py:183
  56.3 0.6 collective-permute-start.4
  56.9 0.1 collective-permute-start.6
  56.9 8.9 %attend.2 = (bf16[192,2048]{1,0:T(8,128)(2,1)S(1)}, bf16[2,192,1024]{2,1,0:T(8,128)(2,1)}, f32[3,2,256]{2,1,0:T(2,128)S(1)}) custom-call(f32[12,28]{1,0:T(8,128)S(1)} %broadcast_select_fusion.named_hbm, bf16[2,3,64,1024]{3,2,1,0:T(8,128)(2,1)} %bitcast.56, bf16[2,3,64,1024]{3,2,1,0:T(8,128)(2,1)} %bitcast.54, bf16[768,256]{1,0:T(8,128)(2,1)S(1)} %latents.1.own_hbm, ...), custom_call_target="tpu_custom_call" | custom-call | flops 4429185024 | bytes 9306112 | tf_op jit(solution)/shard_map/attend/pallas_call | solution.py:419
  65.9 0.5 collective-permute-start.5
  66.5 0.0 collective-permute-done.6
  66.5 0.8 %collective-permute-done.5 = f32[3,256]{1,0:T(4,128)S(1)} collective-permute-done((f32[3,256]{1,0:T(4,128)S(1)}, f32[3,256]{1,0:T(4,128)S(1)}, u32[]{:S(2)}, u32[]{:S(2)}) %collective-permute-start.5) | collective-permute-done | bytes 3104 | tf_op jit(solution)/shard_map/ppermute | solution.py:512
  67.3 0.1 reshape.96
  67.4 0.7 reshape.97
  68.1 0.0 collective-permute-done.3.refs_0_
  68.1 1.9 %collective-permute-done.4.refs_1_ = bf16[192,1024]{1,0:T(8,128)(2,1)S(1)} collective-permute-done((bf16[192,1024]{1,0:T(8,128)(2,1)S(1)}, bf16[192,1024]{1,0:T(8,128)(2,1)S(1)}, u32[]{:S(2)}, u32[]{:S(2)}) %collective-permute-start.4) | collective-permute-done | bytes 393248 | tf_op jit(solution)/shard_map/ppermute | solution.py:523
  70.0 1.0 %finish.1 = bf16[192,2048]{1,0:T(8,128)(2,1)} custom-call(bf16[192,2048]{1,0:T(8,128)(2,1)S(1)} %get-tuple-element.15.own_ref, bf16[192,1024]{1,0:T(8,128)(2,1)S(1)} %collective-permute-done.3.refs_0_, bf16[192,1024]{1,0:T(8,128)(2,1)S(1)} %collective-permute-done.4.refs_1_), custom_call_target="tpu_custom_call" | custom-call | tf_op jit(solution)/shard_map/finish/pallas_call | solution.py:224
  (14 shorter events, 0.1 us)
Async XLA Ops:
  0.6 1.9 %copy-start = (bf16[768,2048]{1,0:T(8,128)(2,1)S(1)}, bf16[768,2048]{1,0:T(8,128)(2,1)}, u32[]{:S(2)}) copy-start(bf16[768,2048]{1,0:T(8,128)(2,1)} %tok_ref.1) | copy-start | bytes 9437188
  2.5 1.2 %copy-start.1 = (bf16[2048,256]{1,0:T(8,128)(2,1)S(1)}, bf16[2048,256]{1,0:T(8,128)(2,1)}, u32[]{:S(2)}) copy-start(bf16[2048,256]{1,0:T(8,128)(2,1)} %w_ref.1) | copy-start | bytes 3145732
  3.7 0.7 copy-start.3
  5.5 36.5 %collective-permute-start.2 = (bf16[1024,2048]{1,0:T(8,128)(2,1)}, bf16[1024,2048]{1,0:T(8,128)(2,1)}, u32[]{:S(2)}, u32[]{:S(2)}) collective-permute-start(bf16[1024,2048]{1,0:T(8,128)(2,1)} %wa_hbm.5), channel_id=1, source_target_pairs={{0,1},{1,0},{2,3},{3,2},{4,5},{5,4},{6,7},{7,6},{8,9},{9,8},{10,11... | collective-permute-start | bytes 12582920 | tf_op jit(solution)/shard_map/ppermute | solution.py:485
  6.1 6.7 %copy-start.4 = (s32[12,32]{1,0:T(8,128)S(1)}, s32[12,32]{1,0:T(8,128)}, u32[]{:S(2)}) copy-start(s32[12,32]{1,0:T(8,128)} %param.11) | copy-start | bytes 4612
  12.7 29.3 %collective-permute-start = (bf16[384,1024]{1,0:T(8,128)(2,1)}, bf16[384,1024]{1,0:T(8,128)(2,1)S(1)}, u32[]{:S(2)}, u32[]{:S(2)}) collective-permute-start(bf16[384,1024]{1,0:T(8,128)(2,1)} %get-tuple-element.12), channel_id=1, source_target_pairs={{0,1},{1,0},{2,3},{3,2},{4,5},{5,4},{6,7},{7,6},{8,9},{9,8},{10,11... | collective-permute-start | bytes 2359304 | tf_op jit(solution)/shard_map/ppermute | solution.py:495
  13.8 13.7 %all-to-all-start = ((s32[8,1,2]{2,1,0:T(1,128)}), s32[8,1,2]{2,1,0:T(1,128)S(1)}, u32[]{:S(2)}, u32[]{:S(2)}) async-start(s32[8,1,2]{2,1,0:T(1,128)} %copy.21), calls=%async_computation | async-start | bytes 8192 | tf_op jit(solution)/shard_map/all_to_all | solution.py:481
  28.9 11.6 %all-to-all-start.1 = ((bf16[8,2,32,256]{3,2,1,0:T(8,128)(2,1)}), bf16[8,2,32,256]{3,2,1,0:T(8,128)(2,1)S(1)}, u32[]{:S(2)}, u32[]{:S(2)}) async-start(bf16[8,2,32,256]{3,2,1,0:T(8,128)(2,1)} %pick.1), calls=%async_computation.1 | async-start | bytes 524288 | tf_op jit(solution)/shard_map/all_to_all | solution.py:489
  40.5 1.5 %collective-permute-start.1 = (bf16[512,256]{1,0:T(8,128)(2,1)S(1)}, bf16[512,256]{1,0:T(8,128)(2,1)S(1)}, u32[]{:S(2)}, u32[]{:S(2)}) collective-permute-start(bf16[512,256]{1,0:T(8,128)(2,1)S(1)} %bitcast.45), channel_id=1, source_target_pairs={{0,1},{1,0},{2,3},{3,2},{4,5},{5,4},{6,7},{7,6},{8,9},{9,8},{10,11... | collective-permute-start | bytes 786440 | tf_op jit(solution)/shard_map/ppermute | solution.py:493
  42.0 0.9 %copy-start.5 = (bf16[384,1024]{1,0:T(8,128)(2,1)}, bf16[384,1024]{1,0:T(8,128)(2,1)S(1)}, u32[]{:S(2)}) copy-start(bf16[384,1024]{1,0:T(8,128)(2,1)S(1)} %collective-permute-done) | copy-start | bytes 2359300
  50.3 17.8 %collective-permute-start.3 = (bf16[192,1024]{1,0:T(8,128)(2,1)S(1)}, bf16[192,1024]{1,0:T(8,128)(2,1)S(1)}, u32[]{:S(2)}, u32[]{:S(2)}) collective-permute-start(bf16[192,1024]{1,0:T(8,128)(2,1)S(1)} %get-tuple-element.16), channel_id=1, source_target_pairs={{0,2},{1,3},{2,0},{3,1},{4,6},{5,7},{6,4},{7,5},{8,10},{9,11},{10,... | collective-permute-start | bytes 1179656 | tf_op jit(solution)/shard_map/ppermute | solution.py:521
  51.9 1.1 %copy-start.2 = (bf16[2,192,1024]{2,1,0:T(8,128)(2,1)S(1)}, bf16[2,192,1024]{2,1,0:T(8,128)(2,1)}, u32[]{:S(2)}) copy-start(bf16[2,192,1024]{2,1,0:T(8,128)(2,1)} %get-tuple-element.17.ho_hbm) | copy-start | bytes 2359300
  56.3 13.7 %collective-permute-start.4 = (bf16[192,1024]{1,0:T(8,128)(2,1)S(1)}, bf16[192,1024]{1,0:T(8,128)(2,1)S(1)}, u32[]{:S(2)}, u32[]{:S(2)}) collective-permute-start(bf16[192,1024]{1,0:T(8,128)(2,1)S(1)} %project.1), channel_id=1, source_target_pairs={{0,2},{1,3},{2,0},{3,1},{4,6},{5,7},{6,4},{7,5},{8,10},{9,11},{10,... | collective-permute-start | bytes 1179656 | tf_op jit(solution)/shard_map/ppermute | solution.py:523
  56.9 9.6 %collective-permute-start.6 = (f32[3,256]{1,0:T(4,128)S(1)}, f32[3,256]{1,0:T(4,128)S(1)}, u32[]{:S(2)}, u32[]{:S(2)}) collective-permute-start(f32[3,256]{1,0:T(4,128)S(1)} %bitcast.52), channel_id=1, source_target_pairs={{0,1},{1,0},{2,3},{3,2},{4,5},{5,4},{6,7},{7,6},{8,9},{9,8},{10,11... | collective-permute-start | bytes 9224 | tf_op jit(solution)/shard_map/ppermute | solution.py:512
  65.9 1.4 %collective-permute-start.5 = (f32[3,256]{1,0:T(4,128)S(1)}, f32[3,256]{1,0:T(4,128)S(1)}, u32[]{:S(2)}, u32[]{:S(2)}) collective-permute-start(f32[3,256]{1,0:T(4,128)S(1)} %slice_bitcast_fusion), channel_id=1, source_target_pairs={{0,1},{1,0},{2,3},{3,2},{4,5},{5,4},{6,7},{7,6},{8,9},{9,8},{10,11... | collective-permute-start | bytes 9224 | tf_op jit(solution)/shard_map/ppermute | solution.py:512
